TPU v7x, 128 devices: a whole 4x4x4 slice. The times are simulated.
128 devices in a mesh: ep: 64 (over z, y, x), tp: 2 (over core).
Axes of the slice: x: 4, y: 4, z: 4, core: 2. Of those that a mesh axis runs over, the one named last changes fastest.
Arguments:
- tokens: bfloat16 [256, 4096], P('ep'), may hold values from -6 to 6
- memory: float32 [256, 8, 256, 512], P('ep', 'tp'), may hold values from -6 to 6
- normalizer: float32 [256, 8, 256], P('ep', 'tp'), may hold values from -6 to 6
- stabilizer: float32 [256, 8], P('ep', 'tp'), may hold values from -4 to 4
- norm_gain: float32 [4096], replicated, may hold values from 0.1 to 1.9
- w_query: bfloat16 [4096, 8, 256], P(None, 'tp', 'ep'), may hold values from -0.09375 to 0.09375
- w_key: bfloat16 [4096, 8, 256], P(None, 'tp', 'ep'), may hold values from -0.09375 to 0.09375
- w_value: bfloat16 [4096, 8, 512], P(None, 'tp', 'ep'), may hold values from -0.09375 to 0.09375
- w_outgate: bfloat16 [4096, 8, 512], P(None, 'tp', 'ep'), may hold values from -0.09375 to 0.09375
- w_input: bfloat16 [4096, 8], P(None, 'tp'), may hold values from -0.09375 to 0.09375
- w_forget: bfloat16 [4096, 8], P(None, 'tp'), may hold values from -0.09375 to 0.09375
- forget_bias: float32 [8], P('tp'), may hold values from 0 to 4
- w_out: bfloat16 [4096, 4096], P('tp', 'ep'), may hold values from -0.09375 to 0.09375
- ffn_gain: float32 [4096], replicated, may hold values from 0.1 to 1.9
- w_gate: bfloat16 [64, 4096, 512], P('ep', None, 'tp'), may hold values from -0.09375 to 0.09375
- w_up: bfloat16 [64, 4096, 512], P('ep', None, 'tp'), may hold values from -0.09375 to 0.09375
- w_down: bfloat16 [64, 512, 4096], P('ep', 'tp'), may hold values from -0.25 to 0.25
- expert_ids: int32 [256, 2], P('ep'), may hold values from 0 to 63, as said below
- route_weights: float32 [256, 2], P('ep'), may hold values from 0.1 to 1
Outputs:
- out: bfloat16 [256, 4096], P('ep')
- memory_next: float32 [256, 8, 256, 512], P('ep', 'tp')
- normalizer_next: float32 [256, 8, 256], P('ep', 'tp')
- stabilizer_next: float32 [256, 8], P('ep', 'tp')
Inputs may be any that keep to these rules, and one draw needn't show every extreme that they name: `expert_ids`: the 2 experts of a token differ and lie in one group of 8 consecutive experts. Beyond that, any choice is allowed: for instance, all 4 tokens of one index of ep may name the same expert.
All inputs are finite; a program needn't handle non-finite values.
Results may differ from a plain program's by a relative error of at most 0.013.
Values may be sent and summed in bfloat16 or wider, within the bound.
A program may use at most 128 MiB of HBM per device.

v0:
```python
import jax
import jax.numpy as jnp
from jax import lax
from jax.sharding import PartitionSpec as P


def in_one_piece(arrays, axis, split_dim, concat_dim, along):
    widths = [a.shape[along] for a in arrays]
    both = jnp.concatenate(arrays, axis=along)
    whole = lax.all_to_all(both, axis, split_axis=split_dim, concat_axis=concat_dim, tiled=True)
    return tuple(jnp.split(whole, [sum(widths[:k]) for k in range(1, len(widths))], axis=along))


def joined_along(parts, dim):
    dims = list(parts.shape[1:])
    dims[dim] *= parts.shape[0]
    return jnp.moveaxis(parts, 0, dim).reshape(dims)


def from_everyone(shard, axis):
    size = lax.axis_size(axis)
    return lax.all_to_all(
        jnp.broadcast_to(shard[None], (size, *shard.shape)), axis, 0, 0, tiled=True
    )


def gather_directly(shard, axis, dim):
    return joined_along(from_everyone(shard, axis), dim)


def taken_together(shard, axis):
    return from_everyone(shard, axis).astype(jnp.float32).sum(axis=0)


def in_blocks(shard, dim, size):
    before, after = (shard.shape[:dim], shard.shape[dim + 1 :])
    return jnp.moveaxis(shard.reshape(*before, size, -1, *after), dim, 0)


def summed_on_arrival(shard, axis, dim):
    parts = in_blocks(shard, dim, lax.axis_size(axis))
    arrived = lax.all_to_all(parts, axis, split_axis=0, concat_axis=0, tiled=True)
    return arrived.astype(jnp.float32).sum(axis=0)


def rms_scale(values, gain):
    return values * lax.rsqrt(jnp.mean(values * values, axis=-1, keepdims=True) + 1e-06) * gain


def product(left, right):
    return jnp.dot(left, right, preferred_element_type=jnp.float32)


def rounded_term(values):
    return lax.optimization_barrier(values.astype(jnp.bfloat16)).astype(jnp.float32)


def body(
    tokens,
    memory,
    normalizer,
    stabilizer,
    norm_gain,
    w_query,
    w_key,
    w_value,
    w_outgate,
    w_input,
    w_forget,
    forget_bias,
    w_out,
    ffn_gain,
    w_gate,
    w_up,
    w_down,
    expert_ids,
    route_weights,
):
    seqs, width = tokens.shape
    heads, key_size, value_size = (memory.shape[1], memory.shape[2], memory.shape[3])
    value_width = heads * value_size
    key_piece = w_query.shape[2]
    value_piece = w_value.shape[2]
    query_cols = w_query.reshape(width, heads * key_piece)
    key_cols = w_key.reshape(width, heads * key_piece)
    value_cols = w_value.reshape(width, heads * value_piece)
    outgate_cols = w_outgate.reshape(width, heads * value_piece)
    normed = rms_scale(tokens.astype(jnp.float32), norm_gain).astype(jnp.bfloat16)
    piece = lax.all_gather(normed, "ep", axis=0, tiled=True)
    projected = jnp.concatenate(
        [
            product(piece, query_cols),
            product(piece, key_cols),
            product(piece, value_cols),
            product(piece, outgate_cols),
        ],
        axis=1,
    ).astype(jnp.bfloat16)
    all_rows = projected.shape[0]
    narrow = heads * key_piece
    broad = heads * value_piece
    query_part = projected[:, :narrow].reshape(all_rows, heads, key_piece)
    key_part = projected[:, narrow : 2 * narrow].reshape(all_rows, heads, key_piece)
    value_part = projected[:, 2 * narrow : 2 * narrow + broad].reshape(all_rows, heads, value_piece)
    outgate_part = projected[:, 2 * narrow + broad :].reshape(all_rows, heads, value_piece)
    query, key, value, outgate = (
        *in_one_piece((query_part, key_part), "ep", 0, 2, 1),
        *in_one_piece((value_part, outgate_part), "ep", 0, 2, 1),
    )
    in_pre = product(normed, w_input)
    log_forget = jax.nn.log_sigmoid(product(normed, w_forget) + forget_bias)
    scaled = query.astype(jnp.float32) * key_size ** (-0.5)
    key_heads = key.astype(jnp.float32)
    value_heads = value.astype(jnp.float32)
    stab_next = jnp.maximum(log_forget + stabilizer, in_pre)
    decay = jnp.exp(log_forget + stabilizer - stab_next)
    inweight = jnp.exp(in_pre - stab_next)
    memory_next = decay[:, :, None, None] * memory + inweight[:, :, None, None] * (
        key_heads[:, :, :, None] * value_heads[:, :, None, :]
    )
    normalizer_next = decay[:, :, None] * normalizer + inweight[:, :, None] * key_heads
    numerator = jnp.einsum("shd,shde->she", scaled, memory_next, precision=lax.Precision.HIGHEST)
    denominator = jnp.sum(scaled * normalizer_next, axis=-1)
    hidden = numerator / jnp.maximum(jnp.abs(denominator), jnp.exp(-stab_next))[:, :, None]
    hidden = (
        hidden.reshape(seqs, value_width)
        * jax.nn.sigmoid(outgate.reshape(seqs, value_width).astype(jnp.float32))
    ).astype(jnp.bfloat16)
    partial_value = product(gather_directly(hidden, "ep", 0), w_out)
    summed = taken_together(rounded_term(partial_value).astype(jnp.bfloat16), "tp").astype(
        jnp.float32
    )
    mixed = lax.all_to_all(
        summed.astype(jnp.bfloat16), "ep", split_axis=0, concat_axis=1, tiled=True
    )
    resid = tokens.astype(jnp.float32) + mixed.astype(jnp.float32)
    ffn_in = rms_scale(resid, ffn_gain).astype(jnp.bfloat16)
    gate_local, up_local, down_local = (w_gate[0], w_up[0], w_down[0])
    n_experts = lax.axis_size("ep") * w_gate.shape[0]
    piece = lax.all_gather(ffn_in, "ep", axis=0, tiled=True)
    gate_part = product(piece, gate_local)
    up_part = product(piece, up_local)
    act = (jax.nn.silu(gate_part) * up_part).astype(jnp.bfloat16)
    expert_terms = rounded_term(product(act, down_local))
    labels = jnp.arange(n_experts, dtype=jnp.int32)
    route_dense = jnp.sum(
        jnp.where(expert_ids[:, :, None] == labels[None, None, :], route_weights[:, :, None], 0.0),
        axis=1,
    )
    my_weight = lax.all_to_all(route_dense, "ep", split_axis=1, concat_axis=0, tiled=True)
    contrib = expert_terms * my_weight
    halves = summed_on_arrival(contrib.astype(jnp.bfloat16), "tp", 1)
    mine = summed_on_arrival(halves.astype(jnp.bfloat16), "ep", 0)
    ffn_out = gather_directly(mine.astype(jnp.bfloat16), "tp", 1).astype(mine.dtype)
    out = (resid + ffn_out).astype(jnp.bfloat16)
    return (out, memory_next, normalizer_next, stab_next)


def solution(mesh):
    return jax.shard_map(
        body,
        mesh=mesh,
        in_specs=(
            P("ep", None),
            P("ep", "tp", None, None),
            P("ep", "tp", None),
            P("ep", "tp"),
            P(),
            P(None, "tp", "ep"),
            P(None, "tp", "ep"),
            P(None, "tp", "ep"),
            P(None, "tp", "ep"),
            P(None, "tp"),
            P(None, "tp"),
            P("tp"),
            P("tp", "ep"),
            P(),
            P("ep", None, "tp"),
            P("ep", None, "tp"),
            P("ep", "tp", None),
            P("ep", None),
            P("ep", None),
        ),
        out_specs=(P("ep", None), P("ep", "tp", None, None), P("ep", "tp", None), P("ep", "tp")),
        check_vma=False,
    )
```

profile of v0, /device:TPU:1, one launch (start us, length us, event | category | flops | bytes accessed | tf_op | source)
XLA Modules:
  0.0 299.4 jit_solution(17854761620672620778)
XLA Ops:
  7.2 1.0 fusion.25
  8.3 1.5 fusion.51
  9.8 0.9 reshape.107
  10.7 0.9 reshape.109
  11.7 0.8 fusion.27
  12.5 0.9 fusion.32
  13.5 0.9 subtract_exponential_fusion
  14.4 0.8 broadcast_multiply_fusion
  15.4 62.9 %all-gather.5.cloned.1.call-done = bf16[64,4,4096]{2,1,0:T(4,128)(2,1)} async-done(((bf16[1,4,4096]{2,1,0:T(4,128)(2,1)}), bf16[64,4,4096]{2,1,0:T(4,128)(2,1)}) %all-gather.5.cloned.1.call-update) | async-done | bytes 2097168 | tf_op jit(solution)/shard_map/all_gather | solution.py:89
  78.4 3.9 %reshape.126 = bf16[256,4096]{1,0:T(8,128)(2,1)} reshape(bf16[64,4,4096]{2,1,0:T(4,128)(2,1)} %all-gather.5.cloned.1.call-done) | data formatting | bytes 4194304
  82.3 2.5 fusion.14
  84.8 0.7 fusion.13
  85.5 0.7 convolution_convert_fusion.5
  86.2 2.2 convolution_convert_fusion.4
  89.0 1.1 pad_maximum_fusion
  90.0 6.4 %all-to-all-start = ((bf16[256,8,4]{1,2,0:T(4,128)(2,1)}), bf16[256,8,4]{1,2,0:T(4,128)(2,1)S(1)}, u32[]{:S(2)}, u32[]{:S(2)}) async-start(bf16[256,8,4]{1,2,0:T(4,128)(2,1)} %pad_maximum_fusion), calls=%async_computation | async-start | bytes 524288 | tf_op jit(solution)/shard_map/all_to_all | solution.py:10
  96.8 1.1 reshape.138
  97.9 8.0 %all-to-all-done = bf16[256,8,4]{1,2,0:T(4,128)(2,1)S(1)} async-done(((bf16[256,8,4]{1,2,0:T(4,128)(2,1)}), bf16[256,8,4]{1,2,0:T(4,128)(2,1)S(1)}, u32[]{:S(2)}, u32[]{:S(2)}) %all-to-all-start) | async-done | bytes 16416 | tf_op jit(solution)/shard_map/all_to_all | solution.py:10
  105.9 4.9 %all-to-all-start.1 = ((bf16[64,2,128]{2,1,0:T(2,128)(2,1)}), bf16[64,2,128]{2,1,0:T(2,128)(2,1)S(1)}, u32[]{:S(2)}, u32[]{:S(2)}) async-start(bf16[64,2,128]{2,1,0:T(2,128)(2,1)} %reshape.138), calls=%async_computation.1 | async-start | bytes 65536 | tf_op jit(solution)/shard_map/all_to_all | solution.py:10
  111.4 1.2 multiply_reduce_fusion
  112.8 1.2 copy.115
  114.0 5.1 %all-to-all-done.1 = bf16[64,2,128]{2,1,0:T(2,128)(2,1)S(1)} async-done(((bf16[64,2,128]{2,1,0:T(2,128)(2,1)}), bf16[64,2,128]{2,1,0:T(2,128)(2,1)S(1)}, u32[]{:S(2)}, u32[]{:S(2)}) %all-to-all-start.1) | async-done | bytes 32800 | tf_op jit(solution)/shard_map/all_to_all | solution.py:10
  119.1 0.6 reshape.139
  120.0 0.7 all_to_all.70
  120.6 4.2 %multiply_add_fusion = f32[4,4,256,512]{3,2,1,0:T(8,128)S(1)} fusion(f32[4,4,256,512]{3,2,1,0:T(8,128)} %param.20, f32[4,4,512]{2,1,0:T(4,128)S(1)} %slice_convert_fusion.1, f32[4,4,256]{2,1,0:T(4,128)S(1)} %copy.104, f32[4,4]{1,0:T(4,128)S(1)} %get-tuple-element.30, f32[4,4]{1,0:T(4,128)S(1)} %subtract_exponential_fusion.1), kind=kLoop, calls=%fused_computation | loop fusion | flops 8388608 | bytes 16826496 | tf_op jit(solution)/shard_map/add | solution.py:118
  124.8 4.0 %fusion.34 = f32[4,4,1,512]{3,2,1,0:T(1,128)S(1)} fusion(f32[4,4,256,1]{2,3,1,0:T(1,128)S(1)} %copy.115, f32[4,4,256,512]{3,2,1,0:T(8,128)S(1)} %multiply_add_fusion), kind=kOutput, calls=%fused_computation.63 | convolution fusion | flops 25165824 | bytes 8437760 | tf_op jit(solution)/shard_map/shd,shde->she/dot_general | solution.py:122
  129.0 0.5 broadcast_in_dim.14
  129.5 18.8 %all_to_all.90 = bf16[64,4,2048]{2,1,0:T(4,128)(2,1)S(1)} all-to-all(bf16[64,4,2048]{2,1,0:T(4,128)(2,1)S(1)} %broadcast_in_dim.14), channel_id=1, replica_groups=mesh['ep'=64,'tp'=2] {'ep'}, dimensions={0} | all-to-all | bytes 2097152 | tf_op jit(solution)/shard_map/all_to_all | solution.py:22
  148.3 1.1 reshape.116
  149.4 1.7 convolution_convert_fusion.1
  151.1 9.1 %all_to_all.91 = bf16[2,256,64]{1,2,0:T(8,128)(2,1)S(1)} all-to-all(bf16[2,256,64]{1,2,0:T(8,128)(2,1)S(1)} %broadcast_in_dim.15), channel_id=1, replica_groups=mesh['ep'=64,'tp'=2] {'tp'}, dimensions={0} | all-to-all | bytes 131072 | tf_op jit(solution)/shard_map/all_to_all | solution.py:22
  160.5 12.6 %all_to_all.92 = bf16[64,2,128]{2,1,0:T(2,128)(2,1)S(1)} all-to-all(bf16[64,2,128]{2,1,0:T(2,128)(2,1)S(1)} %reshape.140), channel_id=1, replica_groups=mesh['ep'=64,'tp'=2] {'ep'}, dimensions={0} | all-to-all | bytes 65536 | tf_op jit(solution)/shard_map/all_to_all | solution.py:133
  173.5 0.7 fusion.28
  174.4 12.9 %all_to_all.93 = f32[4,64,1]{0,2,1:T(1,128)S(1)} all-to-all(f32[4,64,1]{0,2,1:T(1,128)S(1)} %copy.111), channel_id=1, replica_groups=mesh['ep'=64,'tp'=2] {'ep'}, dimensions={1} | all-to-all | bytes 2048 | tf_op jit(solution)/shard_map/all_to_all | solution.py:150
  187.5 47.6 %all-gather.7.cloned.1.call-done = bf16[64,4,4096]{2,1,0:T(4,128)(2,1)} async-done(((bf16[1,4,4096]{2,1,0:T(4,128)(2,1)}), bf16[64,4,4096]{2,1,0:T(4,128)(2,1)}) %all-gather.7.cloned.1.call-update) | async-done | bytes 2097168 | tf_op jit(solution)/shard_map/all_gather | solution.py:140
  235.1 3.9 %reshape.128 = bf16[256,4096]{1,0:T(8,128)(2,1)} reshape(bf16[64,4,4096]{2,1,0:T(4,128)(2,1)} %all-gather.7.cloned.1.call-done) | data formatting | bytes 4194304
  239.0 2.9 fusion.3
  242.0 5.9 %convolution_convert_fusion = bf16[256,4096]{1,0:T(8,128)(2,1)} fusion(bf16[1,256,4096]{2,1,0:T(8,128)(2,1)S(1)} %copy-done, bf16[256,4096]{1,0:T(8,128)(2,1)} %reshape.128, bf16[1,4096,256]{2,1,0:T(8,128)(2,1)} %param.34, f32[256,256]{1,0:T(8,128)S(1)} %fusion.3), kind=kOutput, calls=%fused_computation.1 | convolution fusion | flops 1075183616 | bytes 8650752 | tf_op jit(solution)/shard_map/dot_general | solution.py:51
  247.9 2.2 multiply_convert_fusion
  250.3 8.3 %all_to_all.94 = bf16[2,256,2048]{2,1,0:T(8,128)(2,1)} all-to-all(bf16[2,256,2048]{2,1,0:T(8,128)(2,1)S(1)} %bitcast.90), channel_id=1, replica_groups=mesh['ep'=64,'tp'=2] {'tp'}, dimensions={0} | all-to-all | bytes 4194304 | tf_op jit(solution)/shard_map/all_to_all | solution.py:42
  258.6 2.1 reduce_sum.77
  260.7 1.2 reshape.118
  261.9 6.3 %all-to-all-start.7 = ((bf16[64,4,2048]{2,1,0:T(4,128)(2,1)}), bf16[64,4,2048]{2,1,0:T(4,128)(2,1)S(1)}, u32[]{:S(2)}, u32[]{:S(2)}) async-start(bf16[64,4,2048]{2,1,0:T(4,128)(2,1)} %reshape.118), calls=%async_computation.7 | async-start | bytes 2097152 | tf_op jit(solution)/shard_map/all_to_all | solution.py:42
  268.2 1.8 copy.114
  270.0 16.3 %all-to-all-done.7 = bf16[64,4,2048]{2,1,0:T(4,128)(2,1)S(1)} async-done(((bf16[64,4,2048]{2,1,0:T(4,128)(2,1)}), bf16[64,4,2048]{2,1,0:T(4,128)(2,1)S(1)}, u32[]{:S(2)}, u32[]{:S(2)}) %all-to-all-start.7) | async-done | bytes 1048608 | tf_op jit(solution)/shard_map/all_to_all | solution.py:42
  286.3 0.4 reduce_sum.78
  286.8 5.2 %all_to_all.95 = bf16[2,4,2048]{2,1,0:T(4,128)(2,1)S(1)} all-to-all(bf16[2,4,2048]{2,1,0:T(4,128)(2,1)S(1)} %broadcast_in_dim.18), channel_id=1, replica_groups=mesh['ep'=64,'tp'=2] {'tp'}, dimensions={0} | all-to-all | bytes 65536 | tf_op jit(solution)/shard_map/all_to_all | solution.py:22
  291.9 0.6 add_convert_fusion
  (61 shorter events, 3.5 us)
Async XLA Ops:
  7.2 234.8 %copy-start = (bf16[1,256,4096]{2,1,0:T(8,128)(2,1)S(1)}, bf16[1,256,4096]{2,1,0:T(8,128)(2,1)}, u32[]{:S(2)}) copy-start(bf16[1,256,4096]{2,1,0:T(8,128)(2,1)} %param.35) | copy-start | bytes 6291460
  7.2 71.2 %all-gather.5.cloned.1.call-start = ((), (), s32[]{:S(2)}) async-start(), calls=%async_computation.9 | async-start | bytes 2129920 | tf_op jit(solution)/shard_map/all_gather | solution.py:89
  14.4 98.2 %copy-start.8 = (f32[4,4]{1,0:T(4,128)}, f32[4,4]{1,0:T(4,128)S(1)}, u32[]{:S(2)}) copy-start(f32[4,4]{1,0:T(4,128)S(1)} %get-tuple-element.31) | copy-start | bytes 196
  15.4 66.9 %copy-start.4 = (bf16[4096,4,8]{0,2,1:T(8,128)(2,1)S(1)}, bf16[4096,4,8]{0,2,1:T(8,128)(2,1)}, u32[]{:S(2)}) copy-start(bf16[4096,4,8]{0,2,1:T(8,128)(2,1)} %param.27) | copy-start | bytes 786436
  82.3 2.5 copy-start.1
  82.3 2.5 copy-start.5
  90.0 15.9 %all-to-all-start = ((bf16[256,8,4]{1,2,0:T(4,128)(2,1)}), bf16[256,8,4]{1,2,0:T(4,128)(2,1)S(1)}, u32[]{:S(2)}, u32[]{:S(2)}) async-start(bf16[256,8,4]{1,2,0:T(4,128)(2,1)} %pad_maximum_fusion), calls=%async_computation | async-start | bytes 524288 | tf_op jit(solution)/shard_map/all_to_all | solution.py:10
  105.9 13.2 %all-to-all-start.1 = ((bf16[64,2,128]{2,1,0:T(2,128)(2,1)}), bf16[64,2,128]{2,1,0:T(2,128)(2,1)S(1)}, u32[]{:S(2)}, u32[]{:S(2)}) async-start(bf16[64,2,128]{2,1,0:T(2,128)(2,1)} %reshape.138), calls=%async_computation.1 | async-start | bytes 65536 | tf_op jit(solution)/shard_map/all_to_all | solution.py:10
  110.8 124.3 %all-gather.7.cloned.1.call-start = ((), (), s32[]{:S(2)}) async-start(), calls=%async_computation.10 | async-start | bytes 2129920 | tf_op jit(solution)/shard_map/all_gather | solution.py:140
  124.8 4.1 %copy-start.2 = (f32[4,4,256,512]{3,2,1,0:T(8,128)}, f32[4,4,256,512]{3,2,1,0:T(8,128)S(1)}, u32[]{:S(2)}) copy-start(f32[4,4,256,512]{3,2,1,0:T(8,128)S(1)} %multiply_add_fusion) | copy-start | bytes 25165828
  129.5 19.9 %copy-start.6 = (bf16[2048,64]{0,1:T(8,128)(2,1)S(1)}, bf16[2048,64]{0,1:T(8,128)(2,1)}, u32[]{:S(2)}) copy-start(bf16[2048,64]{0,1:T(8,128)(2,1)} %param.31) | copy-start | bytes 786436
  148.3 25.0 %copy-start.3 = (bf16[4,4096]{1,0:T(4,128)(2,1)S(1)}, bf16[4,4096]{1,0:T(4,128)(2,1)}, u32[]{:S(2)}) copy-start(bf16[4,4096]{1,0:T(4,128)(2,1)} %param.19) | copy-start | bytes 98308
  148.3 25.2 %copy-start.7 = (f32[4096]{0:T(1024)S(1)}, f32[4096]{0:T(1024)}, u32[]{:S(2)}) copy-start(f32[4096]{0:T(1024)} %param.32) | copy-start | bytes 49156
  148.3 25.9 %copy-start.9 = (f32[4,2]{0,1:T(2,128)S(1)}, f32[4,2]{0,1:T(2,128)}, u32[]{:S(2)}) copy-start(f32[4,2]{0,1:T(2,128)} %param.37) | copy-start | bytes 100
  148.3 25.9 %copy-start.10 = (s32[4,2]{0,1:T(2,128)S(1)}, s32[4,2]{0,1:T(2,128)}, u32[]{:S(2)}) copy-start(s32[4,2]{0,1:T(2,128)} %param.36) | copy-start | bytes 100
  261.9 24.4 %all-to-all-start.7 = ((bf16[64,4,2048]{2,1,0:T(4,128)(2,1)}), bf16[64,4,2048]{2,1,0:T(4,128)(2,1)S(1)}, u32[]{:S(2)}, u32[]{:S(2)}) async-start(bf16[64,4,2048]{2,1,0:T(4,128)(2,1)} %reshape.118), calls=%async_computation.7 | async-start | bytes 2097152 | tf_op jit(solution)/shard_map/all_to_all | solution.py:42
Sparse Core Ops, SparseCore 0:
  11.4 66.8 all-gather.4
  174.3 60.7 all-gather.6
where the time goes:
time: 301 us; the launch traced here: 299 us
  waiting for transfers between devices  140 us (47%)
  blocking collectives  66.8 us (22%)
  matrix products  22.5 us (7%)
  local copies, waits for them, and re-layouts  20.8 us (7%)
  starting transfers between devices  17.8 us (6%)
  other arithmetic  17.2 us (6%)
  between operations  14.4 us (5%)
    all_gather x1, waiting for transfers between devices, body(): piece = lax.all_gather(normed, 'ep', axis=0, tiled=True)  62.9 us
    all_gather x1, waiting for transfers between devices, body(): piece = lax.all_gather(ffn_in, 'ep', axis=0, tiled=True)  47.6 us
    all_to_all x3, blocking collectives, from_everyone(): lax.all_to_all(jnp.broadcast_to(shard[None], (size, *shard.shape)), axis,...  33.1 us
    dot_general x9, matrix products, product(): return jnp.dot(left, right, preferred_element_type=jnp.float32)  18.4 us
    all_to_all x1, waiting for transfers between devices, summed_on_arrival(): lax.all_to_all(parts, axis, split_axis=0, concat_axis=0, tiled=True)  16.3 us
    all_to_all x2, waiting for transfers between devices, in_one_piece(): lax.all_to_all(both, axis, split_axis=split_dim, concat_axis=concat_dim,...  13.1 us
    all_to_all x1, blocking collectives, body(): lax.all_to_all(route_dense, 'ep', split_axis=1, concat_axis=0, tiled=True)  12.9 us
    all_to_all x1, blocking collectives, body(): lax.all_to_all(summed.astype(jnp.bfloat16), 'ep', split_axis=0, concat_ax...  12.6 us
  transfers between devices with their start and end apart: 5, of which 5 were waited for; matrix products, arithmetic and copies ran while one was open for 4% of the time, Pallas kernels for 0%

commit v1 on v0

v1 whole, which is shorter than its diff:
```python
import functools

import jax
import jax.numpy as jnp
from jax import lax
from jax.experimental import pallas as pl
from jax.experimental.pallas import tpu as pltpu
from jax.sharding import PartitionSpec as P

MESH = pl.DeviceIdType.MESH
F32 = jnp.float32
BF16 = jnp.bfloat16
STRIDE = {"x": 1, "y": 4, "z": 16}
SEND_ORDER = (1, 3, 2)


def place():
    ep = lax.axis_index("ep")
    at = {"x": lax.rem(ep, 4), "y": lax.rem(ep // 4, 4), "z": ep // 16}
    return ep, lax.axis_index("tp"), at


def shifted(at, axis, offset):
    return lax.rem(at[axis] + 4 + offset, 4)


def peer(ep, at, axis, offset):
    return ep + (shifted(at, axis, offset) - at[axis]) * STRIDE[axis]


def remote(src, dst, send, recv, ep, tp):
    return pltpu.make_async_remote_copy(
        src_ref=src, dst_ref=dst, send_sem=send, recv_sem=recv, device_id=(ep, tp), device_id_type=MESH
    )


def greet(ep, tp, at):
    barrier = pltpu.get_barrier_semaphore()
    for axis in "xyz":
        for o in (1, 2, 3):
            pl.semaphore_signal(barrier, inc=1, device_id=(peer(ep, at, axis, o), tp), device_id_type=MESH)
    pl.semaphore_signal(barrier, inc=1, device_id=(ep, 1 - tp), device_id_type=MESH)


def met():
    pl.semaphore_wait(pltpu.get_barrier_semaphore(), 10)


AXES = (("y", "z"), ("z", "y"))


def line_of(at, part, m, n):
    first, second = AXES[part]
    c = {first: shifted(at, first, -m), second: shifted(at, second, -n)}
    return c["z"] * 4 + c["y"]


def spread_x(ep, tp, at, own, slot, s1, r1):
    for o in SEND_ORDER:
        remote(own, slot(at["x"]), s1.at[o], r1.at[o], peer(ep, at, "x", o), tp).start()


def spread_x_wait(ep, tp, at, own, slot, s1, r1):
    for o in SEND_ORDER:
        remote(own, slot(shifted(at, "x", -o)), s1.at[o], r1.at[o], ep, tp).wait_recv()


def spread_x_end(ep, tp, at, own, slot, s1, r1):
    for o in SEND_ORDER:
        remote(own, slot(at["x"]), s1.at[o], r1.at[o], ep, tp).wait_send()


def lines_relay(ep, tp, at, ref, part, m, n, pair):
    if pair is not None:
        here = ref(line_of(at, part, m, n), part)
        remote(here, here, pair[0].at[part, m, n], pair[1].at[part, m, n], ep, 1 - tp).start()


def lines_onward(ep, tp, at, ref, part, m, s3, r3):
    here = ref(line_of(at, part, m, 0), part)
    for o in SEND_ORDER:
        remote(here, here, s3.at[part, m, o], r3.at[part, m, o], peer(ep, at, AXES[part][1], o), tp).start()


def spread_lines_early(ep, tp, at, ref, s2, r2, s3, r3, pair=None):
    for part in range(2):
        here = ref(line_of(at, part, 0, 0), part)
        for o in SEND_ORDER:
            remote(here, here, s2.at[part, o], r2.at[part, o], peer(ep, at, AXES[part][0], o), tp).start()
    for part in range(2):
        lines_onward(ep, tp, at, ref, part, 0, s3, r3)
        lines_relay(ep, tp, at, ref, part, 0, 0, pair)


def spread_lines_late(ep, tp, at, ref, s2, r2, s3, r3, pair=None, seen=None):
    for m in SEND_ORDER:
        for part in range(2):
            here = ref(line_of(at, part, m, 0), part)
            remote(here, here, s2.at[part, m], r2.at[part, m], ep, tp).wait_recv()
            lines_onward(ep, tp, at, ref, part, m, s3, r3)
            lines_relay(ep, tp, at, ref, part, m, 0, pair)
            if seen is not None:
                seen(part, line_of(at, part, m, 0))
    for m in (0, 1, 3, 2):
        for o in SEND_ORDER:
            for part in range(2):
                here = ref(line_of(at, part, m, o), part)
                remote(here, here, s3.at[part, m, o], r3.at[part, m, o], ep, tp).wait_recv()
                lines_relay(ep, tp, at, ref, part, m, o, pair)
                if seen is not None:
                    seen(part, line_of(at, part, m, o))


def spread_lines_pair_wait(ep, tp, at, other, pair):
    for part in range(2):
        for m in range(4):
            for n in range(4):
                here = other(line_of(at, part, m, n), part)
                remote(here, here, pair[0].at[part, m, n], pair[1].at[part, m, n], ep, 1 - tp).wait_recv()


def spread_lines_end(ep, tp, at, ref, s2, r2, s3, r3, pair=None):
    here0 = [ref(line_of(at, part, 0, 0), part) for part in range(2)]
    for part in range(2):
        here = here0[part]
        for o in SEND_ORDER:
            remote(here, here, s2.at[part, o], r2.at[part, o], ep, tp).wait_send()
        for m in range(4):
            for o in SEND_ORDER:
                remote(here, here, s3.at[part, m, o], r3.at[part, m, o], ep, tp).wait_send()
            if pair is not None:
                for n in range(4):
                    remote(here, here, pair[0].at[part, m, n], pair[1].at[part, m, n], ep, 1 - tp).wait_send()


def part_cols(part, width):
    return pl.ds(part * width, width)


def kernel_a(
    tok_ref, gain_ref, ids_ref, rw_ref, wq_hbm, wk_hbm, wv_hbm, wo_hbm,
    recv_ref, all_ref,
    xblk, wq, wk, wv, wo, wt, acc, squares, slab,
    wsem, s1, r1, s2, r2, s3, r3, ps, pr, sa, ra,
):
    ep, tp, at = place()
    greet(ep, tp, at)
    loads = [
        pltpu.make_async_copy(src, dst, wsem.at[n])
        for n, (src, dst) in enumerate(((wq_hbm, wq), (wk_hbm, wk), (wv_hbm, wv), (wo_hbm, wo)))
    ]
    for load in loads:
        load.start()
    half = 2048
    own = tok_ref.at[:, pl.ds(pl.multiple_of(tp * half, 128), half)]
    met()
    slot = lambda x: xblk.at[x]
    spread_x(ep, tp, at, own, slot, s1, r1)
    xblk[at["x"]] = tok_ref[:, pl.ds(pl.multiple_of(tp * half, 128), half)]
    spread_x_wait(ep, tp, at, own, slot, s1, r1)
    mine = at["z"] * 4 + at["y"]
    for n in range(0, half, 512):
        cols = pl.ds(n, 512)
        all_ref[tp, mine, :, cols] = jnp.concatenate([xblk[x, :, cols].astype(F32) for x in range(4)], axis=0).astype(BF16)
    ref = lambda line, part: all_ref.at[tp, line, :, part_cols(part, half // 2)]
    other = lambda line, part: all_ref.at[1 - tp, line, :, part_cols(part, half // 2)]
    lines = (ep, tp, at, ref, s2, r2, s3, r3, (ps, pr))
    spread_lines_early(*lines)
    for load in loads:
        load.wait()
    wt[96:128, :] = jnp.zeros((32, 4096), BF16)
    for n in range(0, 4096, 1024):
        cols = pl.ds(n, 1024)
        for row, tall, w in ((0, 16, wq), (16, 16, wk), (32, 32, wv), (64, 32, wo)):
            wt[row : row + tall, cols] = jnp.concatenate([w[h, :, cols].astype(F32) for h in range(4)], axis=0).astype(BF16)

    squares[...] = jnp.zeros((16, 16, 128), F32)

    def measured(side, part, line):
        total = squares[line]
        for n in range(0, half // 2, 128):
            v = all_ref[side, line, :, pl.ds(part * (half // 2) + n, 128)].astype(F32)
            total += v * v
        squares[line] = total

    for part in range(2):
        measured(tp, part, mine)
    spread_lines_late(*lines, seen=lambda part, line: measured(tp, part, line))
    for part in range(2):
        for m in range(4):
            for n in range(4):
                line = line_of(at, part, m, n)
                here = other(line, part)
                remote(here, here, ps.at[part, m, n], pr.at[part, m, n], ep, 1 - tp).wait_recv()
                measured(1 - tp, part, line)
    mean = jnp.sum(squares[...].reshape(256, 128), axis=-1, keepdims=True) * (1.0 / 4096)
    scale = lax.rsqrt(mean + 1e-06)
    for n in range(0, 4096, 1024):
        cols = pl.ds(n, 1024)
        x = all_ref[n // half, :, :, pl.ds(n % half, 1024)].reshape(256, 1024).astype(F32)
        normed = (x * scale * gain_ref[:, cols]).astype(BF16)
        term = lax.dot_general(normed, wt[:, cols], (((1,), (1,)), ((), ())), preferred_element_type=F32)
        if n == 0:
            acc[...] = term
        else:
            acc[...] += term
    lane = lax.broadcasted_iota(jnp.int32, (4, 128), 1)
    diagonal = lax.broadcasted_iota(jnp.int32, (4, 4), 0) == lax.broadcasted_iota(jnp.int32, (4, 4), 1)
    upright = lambda row: jnp.sum(jnp.where(diagonal, row, 0.0), axis=1, keepdims=True)
    ids = ids_ref[...].astype(F32)
    id0, id1 = upright(ids[0:1]), upright(ids[1:2])
    rw0, rw1 = upright(rw_ref[0:1, :]), upright(rw_ref[1:2, :])
    for pairs in range(32):
        eight = acc[8 * pairs : 8 * pairs + 8, :]
        for k in range(2):
            e = 2 * pairs + k
            weight = jnp.where(id0 == float(e), rw0, 0.0) + jnp.where(id1 == float(e), rw1, 0.0)
            slab[e] = jnp.where(lane < 96, eight[4 * k : 4 * k + 4], jnp.where(lane == 96, weight, 0.0))

    @pl.loop(1, 64)
    def _(o):
        to = ep ^ o
        remote(slab.at[to], recv_ref.at[ep], sa.at[o], ra.at[o], to, tp).start()

    recv_ref[ep] = slab[ep]
    spread_x_end(ep, tp, at, own, slot, s1, r1)
    spread_lines_end(*lines)

    @pl.loop(1, 64)
    def _(o):
        remote(slab.at[ep ^ o], recv_ref.at[ep ^ o], sa.at[o], ra.at[o], ep ^ o, tp).wait()


def log_sigmoid(v):
    return -(jnp.maximum(-v, 0.0) + jnp.log1p(jnp.exp(-jnp.abs(v))))


def one_hot(rows, cols, test):
    r = lax.broadcasted_iota(jnp.int32, (rows, cols), 0)
    c = lax.broadcasted_iota(jnp.int32, (rows, cols), 1)
    return test(r, c)


def kernel_b(
    recv_ref, tok_ref, gain_ref, win_ref, wfg_ref, fbias_ref, stab_ref, nrm_ref, mem_hbm,
    memn_hbm, nrmn_ref, stabn_ref, hid_ref,
    buf, kq, hids, isem, osem,
):
    ins = [pltpu.make_async_copy(mem_hbm.at[n // 4, n % 4], buf.at[n], isem.at[n]) for n in range(16)]
    outs = [pltpu.make_async_copy(buf.at[n], memn_hbm.at[n // 4, n % 4], osem.at[n]) for n in range(16)]
    for copy in ins:
        copy.start()
    x = tok_ref[...].astype(F32)
    scale = lax.rsqrt(jnp.mean(x * x, axis=-1, keepdims=True) + 1e-06)
    normed = (x * scale * gain_ref[...]).astype(BF16).astype(F32)
    lane = lax.broadcasted_iota(jnp.int32, (4, 4), 1)
    in_pre = jnp.zeros((4, 4), F32)
    forget = jnp.zeros((4, 4), F32)
    for h in range(4):
        i_h = jnp.sum(normed * win_ref[h : h + 1, :].astype(F32), axis=-1, keepdims=True)
        f_h = jnp.sum(normed * wfg_ref[h : h + 1, :].astype(F32), axis=-1, keepdims=True)
        in_pre = jnp.where(lane == h, i_h, in_pre)
        forget = jnp.where(lane == h, f_h, forget)
    log_forget = log_sigmoid(forget + fbias_ref[...])
    held = log_forget + stab_ref[...]
    stab_next = jnp.maximum(held, in_pre)
    decay = jnp.exp(held - stab_next)
    inweight = jnp.exp(in_pre - stab_next)
    floor = jnp.exp(-stab_next)
    stabn_ref[...] = stab_next

    e4 = one_hot(256, 64, lambda r, c: r // 4 == c).astype(BF16)
    e8 = one_hot(512, 64, lambda r, c: r // 8 == c).astype(BF16)
    keep4 = one_hot(256, 128, lambda r, c: (r % 4 == c % 4) & (c < 32))
    keep8 = one_hot(512, 128, lambda r, c: (r % 8 == c % 8) & (c >= 32) & (c < 96))
    vo_cols = jnp.zeros((512, 128), F32)
    qk_cols = jnp.zeros((256, 128), F32)
    wide = []
    for h in range(4):
        wide.append(one_hot(128, 256, lambda r, c: (r // 4 == jnp.where(c < 128, 4 + h, h)) & (r < 32)).astype(BF16))
    for t in range(4):
        rows = recv_ref[pl.ds(t, 64, stride=4), :].astype(BF16)
        y4 = jnp.where(keep4, jnp.dot(e4, rows, preferred_element_type=F32), 0.0).astype(BF16)
        y8 = jnp.where(keep8, jnp.dot(e8, rows, preferred_element_type=F32), 0.0).astype(BF16)
        for h in range(4):
            kq[t * 4 + h] = jnp.dot(y4, wide[h], preferred_element_type=F32)
        f4 = one_hot(128, 128, lambda r, c: (c == t * 8 + r // 4) & (r < 32)).astype(BF16)
        f8 = one_hot(128, 128, lambda r, c: (c == t * 8 + (r - 32) // 8) & (r >= 32) & (r < 96)).astype(BF16)
        qk_cols += jnp.dot(y4, f4, preferred_element_type=F32)
        vo_cols += jnp.dot(y8, f8, preferred_element_type=F32)
    qk_rows = qk_cols.T
    vo_rows = vo_cols.T
    for n in range(16):
        t, h = n // 4, n % 4
        d = decay[t : t + 1, h : h + 1]
        w = inweight[t : t + 1, h : h + 1]
        q_row = qk_rows[t * 8 + h : t * 8 + h + 1, :] * 0.0625
        k_row = qk_rows[t * 8 + 4 + h : t * 8 + 5 + h, :]
        v_row = vo_rows[t * 8 + h : t * 8 + h + 1, :]
        o_row = vo_rows[t * 8 + 4 + h : t * 8 + 5 + h, :]
        norm_next = d * nrm_ref[t, h : h + 1, :] + w * k_row
        nrmn_ref[t, h : h + 1, :] = norm_next
        den = jnp.sum(q_row * norm_next, axis=-1, keepdims=True)
        ins[n].wait()
        d_all = jnp.broadcast_to(d, (8, 128))
        vs = [jnp.broadcast_to(w * v_row[:, 128 * c : 128 * c + 128], (8, 128)) for c in range(4)]

        def step(r, total, n=n, d_all=d_all, vs=vs):
            total = list(total)
            for g in range(4):
                rows = pl.ds(pl.multiple_of(r * 32 + 8 * g, 8), 8)
                k_all = kq[n, rows, 0:128]
                q_all = kq[n, rows, 128:256]
                for c in range(4):
                    cols = slice(128 * c, 128 * c + 128)
                    new = d_all * buf[n, rows, cols] + k_all * vs[c]
                    buf[n, rows, cols] = new
                    total[c] = total[c] + q_all * new
            return tuple(total)

        total = lax.fori_loop(0, 8, step, tuple(jnp.zeros((8, 128), F32) for _ in range(4)))
        outs[n].start()
        numer = jnp.sum(jnp.concatenate(total, axis=1), axis=0, keepdims=True) * 0.0625
        hidden = numer / jnp.maximum(jnp.abs(den), floor[t : t + 1, h : h + 1]) * jax.nn.sigmoid(o_row)
        hids[t : t + 1, h * 512 : (h + 1) * 512] = hidden
    hid_ref[...] = hids[...].astype(BF16)
    for copy in outs:
        copy.wait()


def kernel_c(
    hid_ref, recv_ref, gain_ref, tok_hbm, wo_hbm, wg_hbm, wu_hbm, wd_hbm,
    out_ref,
    xblk, hall, wo, toks, wg, wu, wd, pk, pr_in, mall, resid, resid_own, gate, up, act, away, back, terms,
    r1buf, s1buf, r2buf, xsend, xrecv, ends,
    wsem, s1, r1, s2, r2, s3, r3, ms1, mr1, ms2, mr2, ms3, mr3, mps, mpr, dps, dpr, hs, hr,
    q1s, q1r, q2s, q2r, q3s, q3r, fs, fr,
):
    ep, tp, at = place()
    greet(ep, tp, at)
    loads = [
        pltpu.make_async_copy(src, dst, wsem.at[n])
        for n, (src, dst) in enumerate(((wo_hbm, wo), (tok_hbm, toks), (wg_hbm, wg), (wu_hbm, wu), (wd_hbm, wd)))
    ]
    for load in loads:
        load.start()
    half = 2048
    mine = at["z"] * 4 + at["y"]
    met()
    slot = lambda x: xblk.at[x]
    spread_x(ep, tp, at, hid_ref, slot, s1, r1)
    xblk[at["x"]] = hid_ref[...]
    spread_x_wait(ep, tp, at, hid_ref, slot, s1, r1)
    for n in range(0, half, 512):
        cols = pl.ds(n, 512)
        hall[mine, :, cols] = jnp.concatenate([xblk[x, :, cols].astype(F32) for x in range(4)], axis=0).astype(BF16)
    href = lambda line, part: hall.at[line, :, part_cols(part, half // 2)]
    hidden_lines = (ep, tp, at, href, s2, r2, s3, r3)
    spread_lines_early(*hidden_lines)
    for load in loads:
        load.wait()
    spread_lines_late(*hidden_lines)

    term = jnp.zeros((256, 64), F32)
    for n in range(0, half, 512):
        term += lax.dot_general(
            hall[:, :, pl.ds(n, 512)].reshape(256, 512), wo[:, pl.ds(n, 512)],
            (((1,), (1,)), ((), ())), preferred_element_type=F32,
        )
    for p in range(2):
        pk[p] = jnp.concatenate([term[128 * p : 128 * p + 64], term[128 * p + 64 : 128 * p + 128]], axis=1).astype(BF16)
    swap = remote(pk.at[1 - tp], pr_in, hs, hr, ep, 1 - tp)
    swap.start()
    spread_x_end(ep, tp, at, hid_ref, slot, s1, r1)
    spread_lines_end(*hidden_lines)
    swap.wait()
    mall[tp, mine, at["x"]] = (pk[tp].astype(F32) + pr_in[...].astype(F32)).astype(BF16)
    own = mall.at[tp, mine, at["x"]]
    mslot = lambda x: mall.at[tp, mine, x]
    spread_x(ep, tp, at, own, mslot, ms1, mr1)
    spread_x_wait(ep, tp, at, own, mslot, ms1, mr1)
    mref = lambda line, part: mall.at[tp, line, :, pl.ds(32 * part, 32), :]
    mother = lambda line, part: mall.at[1 - tp, line, :, pl.ds(32 * part, 32), :]
    mixed_lines = (ep, tp, at, mref, ms2, mr2, ms3, mr3, (mps, mpr))
    spread_lines_early(*mixed_lines)
    spread_lines_late(*mixed_lines)
    spread_lines_pair_wait(ep, tp, at, mother, (mps, mpr))

    low = lax.broadcasted_iota(jnp.int32, (64, 128), 1) < 64
    scales = []
    for p in range(2):

        def pair_of_chips(jj, sums, p=p):
            a = mall[p, jj // 2, 2 * lax.rem(jj, 2)].astype(F32)
            b = mall[p, jj // 2, 2 * lax.rem(jj, 2) + 1].astype(F32)
            mixes = (jnp.where(low, a, pltpu.roll(b, 64, 1)), jnp.where(low, pltpu.roll(a, 64, 1), b))
            cols = pl.ds(pl.multiple_of(128 * jj, 128), 128)
            tcols = pl.ds(pl.multiple_of(128 * lax.rem(jj, 16), 128), 128)
            new = []
            for k in range(2):
                row = 128 * p + 64 * k
                r = toks[jj // 16, row // 16 : row // 16 + 4, :, tcols].reshape(64, 128).astype(F32) + mixes[k]
                resid[row : row + 64, cols] = r
                new.append(sums[k] + r * r)
            return tuple(new)

        sums = lax.fori_loop(0, 32, pair_of_chips, (jnp.zeros((64, 128), F32), jnp.zeros((64, 128), F32)))
        for k in range(2):
            scales.append(lax.rsqrt(jnp.sum(sums[k], axis=-1, keepdims=True) * (1.0 / 4096) + 1e-06))
    scale = jnp.concatenate(scales, axis=0)
    my_cols = pl.ds(pl.multiple_of(tp * half, 128), half)
    eight = resid[pl.ds(pl.multiple_of(8 * (ep // 2), 8), 8), my_cols]
    resid_own[...] = jnp.where(lax.rem(ep, 2) == 0, eight[0:4], eight[4:8])

    for n in range(0, 4096, 1024):
        cols = pl.ds(n, 1024)
        x = (resid[:, cols] * scale * gain_ref[:, cols]).astype(BF16)
        g = jnp.dot(x, wg[cols, :], preferred_element_type=F32)
        u = jnp.dot(x, wu[cols, :], preferred_element_type=F32)
        if n == 0:
            gate[...] = g
            up[...] = u
        else:
            gate[...] += g
            up[...] += u
    g = gate[...]
    act[...] = (g * jax.nn.sigmoid(g) * up[...]).astype(BF16)
    weight = recv_ref[:, 96:97]

    def weighted(cols):
        t = jnp.dot(act[...], wd[:, cols], preferred_element_type=F32)
        return t.astype(BF16).astype(F32) * weight

    swaps = []
    for n in range(4):
        here = pl.ds(512 * n, 512)
        cols = pl.ds(pl.multiple_of((1 - tp) * half + 512 * n, 128), 512)
        away[:, :, here] = weighted(cols).astype(BF16).reshape(16, 16, 512)
        copy = remote(away.at[:, :, here], back.at[:, :, here], dps.at[n], dpr.at[n], ep, 1 - tp)
        copy.start()
        swaps.append(copy)
    spread_x_end(ep, tp, at, own, mslot, ms1, mr1)
    spread_lines_end(*mixed_lines)
    for n in range(4):
        here = pl.ds(512 * n, 512)
        cols = pl.ds(pl.multiple_of(tp * half + 512 * n, 128), 512)
        mine_term = weighted(cols)
        swaps[n].wait_recv()
        terms[:, :, :, here] = (mine_term + back[:, :, here].reshape(256, 512).astype(F32)).astype(BF16).reshape(4, 4, 16, 512)
        if n % 2 == 1:
            part = n // 2
            axis = ("z", "y")[part]
            for o in SEND_ORDER:
                c = shifted(at, axis, o)
                src = terms.at[c, :, :, part_cols(0, 1024)] if part == 0 else terms.at[:, c, :, part_cols(1, 1024)]
                remote(src, r1buf.at[part, o], q1s.at[part, o], q1r.at[part, o], peer(ep, at, axis, o), tp).start()

    own1 = lambda part, cols: terms[at["z"], :, :, cols] if part == 0 else terms[:, at["y"], :, cols]
    for part in range(2):
        for o in SEND_ORDER:
            remote(s1buf.at[part], r1buf.at[part, o], q1s.at[part, o], q1r.at[part, o], ep, tp).wait_recv()
        for n in range(0, 1024, 256):
            total = own1(part, pl.ds(part * 1024 + n, 256)).astype(F32)
            for o in (1, 2, 3):
                total += r1buf[part, o, :, :, pl.ds(n, 256)].astype(F32)
            s1buf[part, :, :, pl.ds(n, 256)] = total.astype(BF16)
        axis = ("y", "z")[part]
        for o in SEND_ORDER:
            c = shifted(at, axis, o)
            remote(s1buf.at[part, c], r2buf.at[part, o], q2s.at[part, o], q2r.at[part, o], peer(ep, at, axis, o), tp).start()
    for part in range(2):
        for o in SEND_ORDER:
            remote(s1buf.at[part, 0], r2buf.at[part, o], q2s.at[part, o], q2r.at[part, o], ep, tp).wait_recv()
        for n in range(0, 1024, 512):
            total = s1buf[part, at[("y", "z")[part]], :, pl.ds(n, 512)].astype(F32)
            for o in (1, 2, 3):
                total += r2buf[part, o, :, pl.ds(n, 512)].astype(F32)
            for x in range(4):
                xsend[x, :, pl.ds(part * 1024 + n, 512)] = total[4 * x : 4 * x + 4].astype(BF16)
    for o in SEND_ORDER:
        remote(xsend.at[shifted(at, "x", o)], xrecv.at[o], q3s.at[o], q3r.at[o], peer(ep, at, "x", o), tp).start()
    total = xsend[at["x"]].astype(F32)
    for o in SEND_ORDER:
        remote(xsend.at[0], xrecv.at[o], q3s.at[o], q3r.at[o], ep, tp).wait_recv()
        total += xrecv[o].astype(F32)
    ends[tp] = (resid_own[...] + total).astype(BF16)
    last = remote(ends.at[tp], ends.at[tp], fs, fr, ep, 1 - tp)
    last.start()
    for n in range(4):
        swaps[n].wait_send()
    for part in range(2):
        for o in SEND_ORDER:
            remote(s1buf.at[part], r1buf.at[part, o], q1s.at[part, o], q1r.at[part, o], ep, tp).wait_send()
            remote(s1buf.at[part, 0], r2buf.at[part, o], q2s.at[part, o], q2r.at[part, o], ep, tp).wait_send()
    for o in SEND_ORDER:
        remote(xsend.at[0], xrecv.at[o], q3s.at[o], q3r.at[o], ep, tp).wait_send()
    last.wait_send()
    remote(ends.at[1 - tp], ends.at[1 - tp], fs, fr, ep, 1 - tp).wait_recv()
    for k in range(2):
        out_ref[:, k * half : (k + 1) * half] = ends[k]


V = pl.BlockSpec(memory_space=pltpu.VMEM)
ANY = pl.BlockSpec(memory_space=pl.ANY)
DMA = pltpu.SemaphoreType.DMA


def shape(dims, dtype):
    return jax.ShapeDtypeStruct(dims, dtype)


def call_a(tokens, gain, ids, rw, wq, wk, wv, wo):
    return pl.pallas_call(
        kernel_a,
        name="gather_project",
        out_shape=(shape((64, 4, 128), F32), shape((2, 16, 16, 2048), BF16)),
        in_specs=[V, V, V, V, ANY, ANY, ANY, ANY],
        out_specs=(V, V),
        scratch_shapes=[
            pltpu.VMEM((4, 4, 2048), BF16),
            pltpu.VMEM((4, 4, 4096), BF16),
            pltpu.VMEM((4, 4, 4096), BF16),
            pltpu.VMEM((4, 8, 4096), BF16),
            pltpu.VMEM((4, 8, 4096), BF16),
            pltpu.VMEM((128, 4096), BF16),
            pltpu.VMEM((256, 128), F32),
            pltpu.VMEM((16, 16, 128), F32),
            pltpu.VMEM((64, 4, 128), F32),
            DMA((4,)),
            DMA((4,)), DMA((4,)),
            DMA((2, 4)), DMA((2, 4)),
            DMA((2, 4, 4)), DMA((2, 4, 4)),
            DMA((2, 4, 4)), DMA((2, 4, 4)),
            DMA((64,)), DMA((64,)),
        ],
        compiler_params=pltpu.CompilerParams(collective_id=0, has_side_effects=True),
        cost_estimate=pl.CostEstimate(flops=10**9, bytes_accessed=10**7, transcendentals=0),
    )(tokens, gain, ids, rw, wq, wk, wv, wo)


def call_b(recv, tokens, gain, win, wfg, fbias, stab, nrm, mem):
    return pl.pallas_call(
        kernel_b,
        name="cell",
        out_shape=(
            shape(mem.shape, F32), shape(nrm.shape, F32), shape(stab.shape, F32), shape((4, 2048), BF16),
        ),
        in_specs=[V, V, V, V, V, V, V, V, ANY],
        out_specs=(ANY, V, V, V),
        scratch_shapes=[
            pltpu.VMEM((16, 256, 512), F32),
            pltpu.VMEM((16, 256, 256), F32),
            pltpu.VMEM((4, 2048), F32),
            DMA((16,)), DMA((16,)),
        ],
        compiler_params=pltpu.CompilerParams(),
        cost_estimate=pl.CostEstimate(flops=10**8, bytes_accessed=2 * 10**7, transcendentals=0),
    )(recv, tokens, gain, win, wfg, fbias, stab, nrm, mem)


def call_c(hidden, recv, gain, gathered, wo, wg, wu, wd):
    lines = lambda: [DMA((4,)), DMA((4,)), DMA((2, 4)), DMA((2, 4)), DMA((2, 4, 4)), DMA((2, 4, 4))]
    return pl.pallas_call(
        kernel_c,
        name="experts",
        out_shape=shape((4, 4096), BF16),
        in_specs=[V, V, V, ANY, ANY, ANY, ANY, ANY],
        out_specs=V,
        scratch_shapes=[
            pltpu.VMEM((4, 4, 2048), BF16),
            pltpu.VMEM((16, 16, 2048), BF16),
            pltpu.VMEM((64, 2048), BF16),
            pltpu.VMEM((2, 16, 16, 2048), BF16),
            pltpu.VMEM((4096, 256), BF16),
            pltpu.VMEM((4096, 256), BF16),
            pltpu.VMEM((256, 4096), BF16),
            pltpu.VMEM((2, 64, 128), BF16),
            pltpu.VMEM((64, 128), BF16),
            pltpu.VMEM((2, 16, 4, 64, 128), BF16),
            pltpu.VMEM((256, 4096), F32),
            pltpu.VMEM((4, 2048), F32),
            pltpu.VMEM((256, 256), F32),
            pltpu.VMEM((256, 256), F32),
            pltpu.VMEM((256, 256), BF16),
            pltpu.VMEM((16, 16, 2048), BF16),
            pltpu.VMEM((16, 16, 2048), BF16),
            pltpu.VMEM((4, 4, 16, 2048), BF16),
            pltpu.VMEM((2, 4, 4, 16, 1024), BF16),
            pltpu.VMEM((2, 4, 16, 1024), BF16),
            pltpu.VMEM((2, 4, 16, 1024), BF16),
            pltpu.VMEM((4, 4, 2048), BF16),
            pltpu.VMEM((4, 4, 2048), BF16),
            pltpu.VMEM((2, 4, 2048), BF16),
            DMA((5,)),
            *lines(),
            *lines(), DMA((2, 4, 4)), DMA((2, 4, 4)),
            DMA((4,)), DMA((4,)), DMA(()), DMA(()),
            DMA((2, 4)), DMA((2, 4)), DMA((2, 4)), DMA((2, 4)), DMA((4,)), DMA((4,)), DMA(()), DMA(()),
        ],
        compiler_params=pltpu.CompilerParams(collective_id=1, has_side_effects=True),
        cost_estimate=pl.CostEstimate(flops=2 * 10**9, bytes_accessed=10**7, transcendentals=0),
    )(hidden, recv, gain, gathered, wo, wg, wu, wd)


def body(
    tokens, memory, normalizer, stabilizer, norm_gain, w_query, w_key, w_value, w_outgate, w_input, w_forget,
    forget_bias, w_out, ffn_gain, w_gate, w_up, w_down, expert_ids, route_weights,
):
    turned = lambda w: jnp.transpose(w, (1, 2, 0))
    gain = norm_gain.reshape(1, -1)
    recv, gathered = call_a(
        tokens, gain, expert_ids.T, route_weights.T, turned(w_query), turned(w_key), turned(w_value), turned(w_outgate)
    )
    flat = recv.reshape(256, 128)
    memory_next, normalizer_next, stab_next, hidden = call_b(
        flat, tokens, gain, w_input.T, w_forget.T, forget_bias.reshape(1, 4), stabilizer, normalizer, memory
    )
    out = call_c(hidden, flat, ffn_gain.reshape(1, -1), gathered, w_out.T, w_gate[0], w_up[0], w_down[0])
    return (out, memory_next, normalizer_next, stab_next)


def solution(mesh):
    return jax.shard_map(
        body,
        mesh=mesh,
        in_specs=(
            P("ep", None),
            P("ep", "tp", None, None),
            P("ep", "tp", None),
            P("ep", "tp"),
            P(),
            P(None, "tp", "ep"),
            P(None, "tp", "ep"),
            P(None, "tp", "ep"),
            P(None, "tp", "ep"),
            P(None, "tp"),
            P(None, "tp"),
            P("tp"),
            P("tp", "ep"),
            P(),
            P("ep", None, "tp"),
            P("ep", None, "tp"),
            P("ep", "tp", None),
            P("ep", None),
            P("ep", None),
        ),
        out_specs=(P("ep", None), P("ep", "tp", None, None), P("ep", "tp", None), P("ep", "tp")),
        check_vma=False,
    )
```

time: 301 us -> 110 us (0.37)
  waiting for transfers between devices: 140 us -> 0 us
  Pallas kernels: 0 us -> 107 us
  blocking collectives: 66.8 us -> 0 us
  matrix products: 22.5 us -> 0 us
  local copies, waits for them, and re-layouts: 20.8 us -> 1.39 us
  starting transfers between devices: 17.8 us -> 0 us
  other arithmetic: 17.2 us -> 0 us
  between operations: 14.4 us -> 0.66 us
    all_gather x2 -> x0, waiting for transfers between devices: 110 us -> none  [the longest x1 62.9 us: body(): piece = lax.all_gather(normed, 'ep', axis=0, tiled=True)]
    pallas_call x0 -> x3, Pallas kernels: none -> 107 us  [the longest x1 63.1 us: call_c(): pl.pallas_call(kernel_c, name='experts', out_shape=shape((4, 4096), BF16)...]
    all_to_all x6 -> x0, blocking collectives: 66.8 us -> none  [the longest x3 33.1 us: from_everyone(): lax.all_to_all(jnp.broadcast_to(shard[None], (size, *shard.shape)), axis,...]
    all_to_all x3 -> x0, waiting for transfers between devices: 29.4 us -> none  [the longest x1 16.3 us: summed_on_arrival(): lax.all_to_all(parts, axis, split_axis=0, concat_axis=0, tiled=True)]
    dot_general x10 -> x0, matrix products: 22.5 us -> none  [the longest x9 18.4 us: product(): return jnp.dot(left, right, preferred_element_type=jnp.float32)]
    all_to_all x3 -> x0, starting transfers between devices: 17.5 us -> none  [the longest x2 11.3 us: in_one_piece(): lax.all_to_all(both, axis, split_axis=split_dim, concat_axis=concat_dim,...]
    unnamed x30 -> x1, local copies, waits for them, and re-layouts: 11.7 us -> 1.39 us
    reduce_sum x7 -> x0, other arithmetic: 5.01 us -> none  [the longest x2 2.57 us: summed_on_arrival(): return arrived.astype(jnp.float32).sum(axis=0)]
  transfers between devices with their start and end apart: 5 -> 0, of which waited for: 5 -> 0; matrix products, arithmetic and copies ran while one was open for 4% -> 0% of each run, Pallas kernels for 0% -> 0%
where the time goes in v1:
time: 110 us; the launch traced here: 109 us
  Pallas kernels  107 us (97%)
  local copies, waits for them, and re-layouts  1.39 us (1%)
    pallas_call x1, Pallas kernels, call_c(): pl.pallas_call(kernel_c, name='experts', out_shape=shape((4, 4096), BF16)...  63.1 us
    pallas_call x1, Pallas kernels, call_a(): pl.pallas_call(kernel_a, name='gather_project', out_shape=(shape((64, 4,...  34.1 us
    pallas_call x1, Pallas kernels, call_b(): pl.pallas_call(kernel_b, name='cell', out_shape=(shape(mem.shape, F32), s...  10.1 us

profile of v1, /device:TPU:1, one launch (start us, length us, event | category | flops | bytes accessed | tf_op | source)
XLA Modules:
  0.0 109.3 jit_solution(12537188314482692930)
XLA Ops:
  0.6 34.1 %gather_project.1 = (f32[64,4,128]{2,1,0:T(4,128)}, bf16[2,16,16,2048]{3,2,1,0:T(8,128)(2,1)}) custom-call(bf16[4,4096]{1,0:T(4,128)(2,1)} %tok_ref.3, f32[1,4096]{1,0:T(1,128)} %bitcast.24, s32[2,4]{1,0:T(2,128)} %bitcast.32, f32[2,4]{1,0:T(2,128)} %bitcast.33, bf16[4,4,4096]{2,1,0:T(4,128)(2,1)} %bitcast.30, bf16[4,4,4096]{2,1,0:T(4,128)(2,1)} %bitcast.31, ...), custom_call_target="tpu_custom_call" | custom-call | flops 1000000000 | bytes 10000000 | tf_op jit(solution)/shard_map/gather_project/pallas_call | solution.py:513
  34.7 10.1 %cell.1 = (f32[4,4,256,512]{3,2,1,0:T(8,128)}, f32[4,4,256]{2,1,0:T(4,128)}, f32[4,4]{1,0:T(4,128)}, bf16[4,2048]{1,0:T(4,128)(2,1)}) custom-call(f32[256,128]{1,0:T(8,128)} %bitcast.19, bf16[4,4096]{1,0:T(4,128)(2,1)} %tok_ref.3, f32[1,4096]{1,0:T(1,128)} %bitcast.25, bf16[4,4096]{1,0:T(4,128)(2,1)} %bitcast.22, bf16[4,4096]{1,0:T(4,128)(2,1)} %bitcast.23, ...), custom_call_target="tpu_custom_call" | custom-call | flops 100000000 | bytes 20000000 | tf_op jit(solution)/shard_map/cell/pallas_call | solution.py:542
  44.8 63.1 %experts.1 = bf16[4,4096]{1,0:T(4,128)(2,1)} custom-call(bf16[4,2048]{1,0:T(4,128)(2,1)} %get-tuple-element.11.hid_ref, f32[256,128]{1,0:T(8,128)} %bitcast.20, f32[1,4096]{1,0:T(1,128)} %bitcast.26, bf16[2,16,16,2048]{3,2,1,0:T(8,128)(2,1)} %get-tuple-element.12.tok_hbm, bf16[64,2048]{1,0:T(8,128)(2,1)} %bitcast.21, bf16[4096,256]{1,0:T(8,128)(2,1)} %bitcast.16, ...), custom_call_target="tpu_custom_call" | custom-call | flops 2000000000 | bytes 10000000 | tf_op jit(solution)/shard_map/experts/pallas_call | solution.py:563
  108.0 1.4 %copy.24 = bf16[4,4096]{1,0:T(4,128)(2,1)} copy(bf16[4,4096]{1,0:T(4,128)(2,1)} %experts.1) | data formatting | bytes 65536

commit v2 on v1

v2 whole, which is shorter than its diff:
```python
import functools

import jax
import jax.numpy as jnp
from jax import lax
from jax.experimental import pallas as pl
from jax.experimental.pallas import tpu as pltpu
from jax.sharding import PartitionSpec as P

MESH = pl.DeviceIdType.MESH
F32 = jnp.float32
BF16 = jnp.bfloat16
STRIDE = {"x": 1, "y": 4, "z": 16}
SEND_ORDER = (1, 3, 2)


def place():
    ep = lax.axis_index("ep")
    at = {"x": lax.rem(ep, 4), "y": lax.rem(ep // 4, 4), "z": ep // 16}
    return ep, lax.axis_index("tp"), at


def shifted(at, axis, offset):
    return lax.rem(at[axis] + 4 + offset, 4)


def peer(ep, at, axis, offset):
    return ep + (shifted(at, axis, offset) - at[axis]) * STRIDE[axis]


def remote(src, dst, send, recv, ep, tp):
    return pltpu.make_async_remote_copy(
        src_ref=src, dst_ref=dst, send_sem=send, recv_sem=recv, device_id=(ep, tp), device_id_type=MESH
    )


def greet(ep, tp, at):
    barrier = pltpu.get_barrier_semaphore()
    for axis in "xyz":
        for o in (1, 2, 3):
            pl.semaphore_signal(barrier, inc=1, device_id=(peer(ep, at, axis, o), tp), device_id_type=MESH)
    pl.semaphore_signal(barrier, inc=1, device_id=(ep, 1 - tp), device_id_type=MESH)


def met():
    pl.semaphore_wait(pltpu.get_barrier_semaphore(), 10)


ORDERS = (("x", "y", "z"), ("x", "z", "y"), ("y", "z", "x"))
PARTS = ((0, 640), (640, 640), (1280, 768))
TURN = 1280
WIDE = ((0, 1280), (1280, 1280), (2560, 1536))
WIDE_TURN = 2560


def cols_of(part):
    return pl.ds(PARTS[part][0], PARTS[part][1])


def wide_of(part):
    return pl.ds(WIDE[part][0], WIDE[part][1])


def line_of(at, part, m, n):
    first, second, third = ORDERS[part]
    c = dict(at)
    c[second] = shifted(at, second, -m)
    c[third] = shifted(at, third, -n)
    return c["z"] * 4 + (c["y"] if first == "x" else c["x"])


def first_send(ep, tp, at, part, own, slot, s1, r1):
    axis = ORDERS[part][0]
    for o in SEND_ORDER:
        remote(own, slot(at[axis]), s1.at[part, o], r1.at[part, o], peer(ep, at, axis, o), tp).start()


def first_arrived(ep, tp, at, part, own, slot, s1, r1):
    for o in SEND_ORDER:
        remote(own, slot(at[ORDERS[part][0]]), s1.at[part, o], r1.at[part, o], ep, tp).wait_recv()


def first_end(ep, tp, at, part, own, slot, s1, r1):
    for o in SEND_ORDER:
        remote(own, slot(at[ORDERS[part][0]]), s1.at[part, o], r1.at[part, o], ep, tp).wait_send()


def lines_relay(ep, tp, at, ref, part, m, n, pair):
    if pair is not None:
        here = ref(line_of(at, part, m, n), part)
        remote(here, here, pair[0].at[part, m, n], pair[1].at[part, m, n], ep, 1 - tp).start()


def lines_onward(ep, tp, at, ref, part, m, s3, r3):
    here = ref(line_of(at, part, m, 0), part)
    for o in SEND_ORDER:
        remote(here, here, s3.at[part, m, o], r3.at[part, m, o], peer(ep, at, ORDERS[part][2], o), tp).start()


def lines_early(parts, ep, tp, at, ref, s2, r2, s3, r3, pair=None):
    for part in parts:
        here = ref(line_of(at, part, 0, 0), part)
        for o in SEND_ORDER:
            remote(here, here, s2.at[part, o], r2.at[part, o], peer(ep, at, ORDERS[part][1], o), tp).start()
    for part in parts:
        lines_onward(ep, tp, at, ref, part, 0, s3, r3)
        lines_relay(ep, tp, at, ref, part, 0, 0, pair)


def lines_late(parts, ep, tp, at, ref, s2, r2, s3, r3, pair=None, seen=None):
    if seen is not None:
        for part in parts:
            seen(part, line_of(at, part, 0, 0))
    for m in SEND_ORDER:
        for part in parts:
            here = ref(line_of(at, part, m, 0), part)
            remote(here, here, s2.at[part, m], r2.at[part, m], ep, tp).wait_recv()
            lines_onward(ep, tp, at, ref, part, m, s3, r3)
            lines_relay(ep, tp, at, ref, part, m, 0, pair)
            if seen is not None:
                seen(part, line_of(at, part, m, 0))
    for m in (0, 1, 3, 2):
        for o in SEND_ORDER:
            for part in parts:
                here = ref(line_of(at, part, m, o), part)
                remote(here, here, s3.at[part, m, o], r3.at[part, m, o], ep, tp).wait_recv()
                lines_relay(ep, tp, at, ref, part, m, o, pair)
                if seen is not None:
                    seen(part, line_of(at, part, m, o))


def lines_end(parts, ep, tp, at, ref, s2, r2, s3, r3, pair=None):
    for part in parts:
        here = ref(line_of(at, part, 0, 0), part)
        for o in SEND_ORDER:
            remote(here, here, s2.at[part, o], r2.at[part, o], ep, tp).wait_send()
        for m in range(4):
            for o in SEND_ORDER:
                remote(here, here, s3.at[part, m, o], r3.at[part, m, o], ep, tp).wait_send()
            if pair is not None:
                for n in range(4):
                    remote(here, here, pair[0].at[part, m, n], pair[1].at[part, m, n], ep, 1 - tp).wait_send()


def turned_pieces():
    for z in range(4):
        for y in range(4):
            for x in range(4):
                yield 4 * z + y, 2 * x, 4 * z + x, 2 * y


def stacked(blocks, rows):
    return jnp.concatenate([block[r : r + 2] for r in rows for block in blocks], axis=0).astype(BF16)


def kernel_a(
    tok_ref, gain_ref, ids_ref, rw_ref, wq_hbm, wk_hbm, wv_hbm, wo_hbm,
    recv_ref, all_ref,
    own2, xblk, wq, wk, wv, wo, wt, acc, acc_t, squares, squares_t, comb, came, slab,
    wsem, s1, r1, s2, r2, s3, r3, ws, wr, cs, cr, sa, ra,
):
    ep, tp, at = place()
    greet(ep, tp, at)
    loads = [
        pltpu.make_async_copy(src, dst, wsem.at[n])
        for n, (src, dst) in enumerate(((wq_hbm, wq), (wk_hbm, wk), (wv_hbm, wv), (wo_hbm, wo)))
    ]
    for load in loads:
        load.start()
    mine4 = tok_ref[...].astype(F32)
    mine2 = jnp.where(tp == 0, mine4[0:2], mine4[2:4]).astype(BF16)
    own2[...] = mine2
    own = lambda part: own2.at[:, wide_of(part)]
    slot = lambda part: lambda c: xblk.at[c, :, wide_of(part)]
    met()
    for part in range(3):
        first_send(ep, tp, at, part, own(part), slot(part), s1, r1)
    for part in range(3):
        off, width = WIDE[part]
        xblk[at[ORDERS[part][0]], :, wide_of(part)] = mine2[:, off : off + width]
    ref = lambda line, part: all_ref.at[line, :, wide_of(part)]
    lines = (ep, tp, at, ref, s2, r2, s3, r3)

    def stack(part):
        line = line_of(at, part, 0, 0)
        off, width = WIDE[part]
        for n in range(off, off + width, 256):
            cols = pl.ds(n, 256)
            all_ref[line, :, cols] = stacked([xblk[c, :, cols].astype(F32) for c in range(4)], (0,))

    for part in range(3):
        first_arrived(ep, tp, at, part, own(part), slot(part), s1, r1)
        stack(part)
        lines_early((part,), *lines)
    for load in loads:
        load.wait()
    for side in range(2):
        wt[side, 96:128, :] = jnp.zeros((32, 4096), BF16)
    for n in range(0, 4096, 1024):
        cols = pl.ds(n, 1024)
        for row, tall, w in ((0, 16, wq), (16, 16, wk), (32, 32, wv), (64, 32, wo)):
            wt[tp, row : row + tall, cols] = jnp.concatenate([w[h, :, cols].astype(F32) for h in range(4)], axis=0).astype(BF16)
    share = remote(wt.at[tp, pl.ds(0, 96), :], wt.at[tp, pl.ds(0, 96), :], ws, wr, ep, 1 - tp)
    share.start()
    squares[...] = jnp.zeros((16, 8, 128), F32)
    squares_t[...] = jnp.zeros((16, 8, 128), F32)

    def measured(part, line):
        into = squares_t if part == 2 else squares
        off, width = WIDE[part]
        total = into[line]
        for n in range(off, off + width, 128):
            v = all_ref[line, :, pl.ds(n, 128)].astype(F32)
            total += v * v
        into[line] = total

    lines_late((0, 1, 2), *lines, seen=measured)
    for line, row, line_t, row_t in turned_pieces():
        both = squares[line, row : row + 2] + squares_t[line_t, row_t : row_t + 2]
        squares[line, row : row + 2] = both
        squares_t[line_t, row_t : row_t + 2] = both

    def scale_from(sums):
        mean = jnp.sum(sums[...].reshape(128, 128), axis=-1, keepdims=True) * (1.0 / 4096)
        return lax.rsqrt(mean + 1e-06)

    scale, scale_t = scale_from(squares), scale_from(squares_t)
    share.wait_send()
    remote(wt.at[1 - tp, pl.ds(0, 96), :], wt.at[1 - tp, pl.ds(0, 96), :], ws, wr, ep, 1 - tp).wait_recv()

    def project(off, width, rows_scale):
        cols = pl.ds(off, width)
        x = all_ref[:, :, cols].astype(F32).reshape(128, width)
        normed = (x * rows_scale * gain_ref[:, cols]).astype(BF16)
        right = wt[:, :, cols].reshape(256, width)
        return lax.dot_general(normed, right, (((1,), (1,)), ((), ())), preferred_element_type=F32)

    acc[...] = project(0, WIDE_TURN, scale)
    acc_t[...] = project(WIDE_TURN, 1536, scale_t)
    for e, (line, row, line_t, row_t) in enumerate(turned_pieces()):
        a0, b0 = 8 * line + row, 8 * line_t + row_t
        for side in range(2):
            cols = slice(128 * side, 128 * side + 128)
            comb[side, e] = acc[a0 : a0 + 2, cols] + acc_t[b0 : b0 + 2, cols]
    trade = remote(comb.at[1 - tp], came, cs, cr, ep, 1 - tp)
    trade.start()
    lane = lax.broadcasted_iota(jnp.int32, (4, 128), 1)
    diagonal = lax.broadcasted_iota(jnp.int32, (4, 4), 0) == lax.broadcasted_iota(jnp.int32, (4, 4), 1)
    upright = lambda row: jnp.sum(jnp.where(diagonal, row, 0.0), axis=1, keepdims=True)
    ids = ids_ref[...].astype(F32)
    id0, id1 = upright(ids[0:1]), upright(ids[1:2])
    rw0, rw1 = upright(rw_ref[0:1, :]), upright(rw_ref[1:2, :])
    trade.wait()
    for e in range(64):
        here, there = comb[tp, e], came[e]
        columns = jnp.concatenate([jnp.where(tp == 0, here, there), jnp.where(tp == 0, there, here)], axis=0)
        weight = jnp.where(id0 == float(e), rw0, 0.0) + jnp.where(id1 == float(e), rw1, 0.0)
        slab[e] = jnp.where(lane < 96, columns, jnp.where(lane == 96, weight, 0.0))

    @pl.loop(1, 64)
    def _(o):
        to = ep ^ o
        remote(slab.at[to], recv_ref.at[ep], sa.at[o], ra.at[o], to, tp).start()

    recv_ref[ep] = slab[ep]
    for part in range(3):
        first_end(ep, tp, at, part, own(part), slot(part), s1, r1)
    lines_end((0, 1, 2), *lines)
    for z in range(4):
        for n in range(WIDE_TURN, 4096, 256):
            cols = pl.ds(n, 256)
            four = [all_ref[4 * z + x, :, cols].astype(F32) for x in range(4)]
            for y in range(4):
                all_ref[4 * z + y, :, cols] = stacked(four, (2 * y,))

    @pl.loop(1, 64)
    def _(o):
        remote(slab.at[ep ^ o], recv_ref.at[ep ^ o], sa.at[o], ra.at[o], ep ^ o, tp).wait()


def log_sigmoid(v):
    return -(jnp.maximum(-v, 0.0) + jnp.log1p(jnp.exp(-jnp.abs(v))))


def one_hot(rows, cols, test):
    r = lax.broadcasted_iota(jnp.int32, (rows, cols), 0)
    c = lax.broadcasted_iota(jnp.int32, (rows, cols), 1)
    return test(r, c)


def kernel_b(
    recv_ref, tok_ref, gain_ref, win_ref, wfg_ref, fbias_ref, stab_ref, nrm_ref, mem_hbm,
    memn_hbm, nrmn_ref, stabn_ref, hid_ref,
    buf, kq, hids, isem, osem,
):
    ins = [pltpu.make_async_copy(mem_hbm.at[n // 4, n % 4], buf.at[n], isem.at[n]) for n in range(16)]
    outs = [pltpu.make_async_copy(buf.at[n], memn_hbm.at[n // 4, n % 4], osem.at[n]) for n in range(16)]
    for copy in ins:
        copy.start()
    x = tok_ref[...].astype(F32)
    scale = lax.rsqrt(jnp.mean(x * x, axis=-1, keepdims=True) + 1e-06)
    normed = (x * scale * gain_ref[...]).astype(BF16).astype(F32)
    lane = lax.broadcasted_iota(jnp.int32, (4, 4), 1)
    in_pre = jnp.zeros((4, 4), F32)
    forget = jnp.zeros((4, 4), F32)
    for h in range(4):
        i_h = jnp.sum(normed * win_ref[h : h + 1, :].astype(F32), axis=-1, keepdims=True)
        f_h = jnp.sum(normed * wfg_ref[h : h + 1, :].astype(F32), axis=-1, keepdims=True)
        in_pre = jnp.where(lane == h, i_h, in_pre)
        forget = jnp.where(lane == h, f_h, forget)
    log_forget = log_sigmoid(forget + fbias_ref[...])
    held = log_forget + stab_ref[...]
    stab_next = jnp.maximum(held, in_pre)
    decay = jnp.exp(held - stab_next)
    inweight = jnp.exp(in_pre - stab_next)
    floor = jnp.exp(-stab_next)
    stabn_ref[...] = stab_next

    e4 = one_hot(256, 64, lambda r, c: r // 4 == c).astype(BF16)
    e8 = one_hot(512, 64, lambda r, c: r // 8 == c).astype(BF16)
    keep4 = one_hot(256, 128, lambda r, c: (r % 4 == c % 4) & (c < 32))
    keep8 = one_hot(512, 128, lambda r, c: (r % 8 == c % 8) & (c >= 32) & (c < 96))
    vo_cols = jnp.zeros((512, 128), F32)
    qk_cols = jnp.zeros((256, 128), F32)
    wide = []
    for h in range(4):
        wide.append(one_hot(128, 256, lambda r, c: (r // 4 == jnp.where(c < 128, 4 + h, h)) & (r < 32)).astype(BF16))
    for t in range(4):
        rows = recv_ref[pl.ds(t, 64, stride=4), :].astype(BF16)
        y4 = jnp.where(keep4, jnp.dot(e4, rows, preferred_element_type=F32), 0.0).astype(BF16)
        y8 = jnp.where(keep8, jnp.dot(e8, rows, preferred_element_type=F32), 0.0).astype(BF16)
        for h in range(4):
            kq[t * 4 + h] = jnp.dot(y4, wide[h], preferred_element_type=F32)
        f4 = one_hot(128, 128, lambda r, c: (c == t * 8 + r // 4) & (r < 32)).astype(BF16)
        f8 = one_hot(128, 128, lambda r, c: (c == t * 8 + (r - 32) // 8) & (r >= 32) & (r < 96)).astype(BF16)
        qk_cols += jnp.dot(y4, f4, preferred_element_type=F32)
        vo_cols += jnp.dot(y8, f8, preferred_element_type=F32)
    qk_rows = qk_cols.T
    vo_rows = vo_cols.T
    for n in range(16):
        t, h = n // 4, n % 4
        d = decay[t : t + 1, h : h + 1]
        w = inweight[t : t + 1, h : h + 1]
        q_row = qk_rows[t * 8 + h : t * 8 + h + 1, :] * 0.0625
        k_row = qk_rows[t * 8 + 4 + h : t * 8 + 5 + h, :]
        v_row = vo_rows[t * 8 + h : t * 8 + h + 1, :]
        o_row = vo_rows[t * 8 + 4 + h : t * 8 + 5 + h, :]
        norm_next = d * nrm_ref[t, h : h + 1, :] + w * k_row
        nrmn_ref[t, h : h + 1, :] = norm_next
        den = jnp.sum(q_row * norm_next, axis=-1, keepdims=True)
        ins[n].wait()
        d_all = jnp.broadcast_to(d, (8, 128))
        vs = [jnp.broadcast_to(w * v_row[:, 128 * c : 128 * c + 128], (8, 128)) for c in range(4)]

        def step(r, total, n=n, d_all=d_all, vs=vs):
            total = list(total)
            for g in range(4):
                rows = pl.ds(pl.multiple_of(r * 32 + 8 * g, 8), 8)
                k_all = kq[n, rows, 0:128]
                q_all = kq[n, rows, 128:256]
                for c in range(4):
                    cols = slice(128 * c, 128 * c + 128)
                    new = d_all * buf[n, rows, cols] + k_all * vs[c]
                    buf[n, rows, cols] = new
                    total[c] = total[c] + q_all * new
            return tuple(total)

        total = lax.fori_loop(0, 8, step, tuple(jnp.zeros((8, 128), F32) for _ in range(4)), unroll=True)
        outs[n].start()
        numer = jnp.sum(jnp.concatenate(total, axis=1), axis=0, keepdims=True) * 0.0625
        hidden = numer / jnp.maximum(jnp.abs(den), floor[t : t + 1, h : h + 1]) * jax.nn.sigmoid(o_row)
        hids[t : t + 1, h * 512 : (h + 1) * 512] = hidden
    hid_ref[...] = hids[...].astype(BF16)
    for copy in outs:
        copy.wait()


def kernel_c(
    hid_ref, recv_ref, gain_ref, tok_hbm, wo_hbm, wg_hbm, wu_hbm, wd_hbm,
    out_ref,
    xblk, hall, wo, toks, wg, wu, wd, pre, pre_t, pk, pr_in, mall, resid, squares, gate, up, act, act_t,
    weights, weights_t, terms, r1buf, s1buf, r2buf, xsend, xrecv, ends,
    wsem, s1, r1, s2, r2, s3, r3, ms1, mr1, ms2, mr2, ms3, mr3, es, er, hs, hr,
    q1s, q1r, q2s, q2r, q3s, q3r, fs, fr,
):
    ep, tp, at = place()
    greet(ep, tp, at)
    shared = ((wg_hbm, wg), (wu_hbm, wu), (wd_hbm, wd))
    loads = [pltpu.make_async_copy(wo_hbm, wo, wsem.at[0]), pltpu.make_async_copy(tok_hbm, toks, wsem.at[1])]
    loads += [pltpu.make_async_copy(src, dst.at[tp], wsem.at[2 + n]) for n, (src, dst) in enumerate(shared)]
    for load in loads:
        load.start()
    own = lambda part: hid_ref.at[:, cols_of(part)]
    slot = lambda part: lambda c: xblk.at[c, :, cols_of(part)]
    met()
    for part in range(3):
        first_send(ep, tp, at, part, own(part), slot(part), s1, r1)
    gifts = [remote(src, dst.at[tp], es.at[n], er.at[n], ep, 1 - tp) for n, (src, dst) in enumerate(shared)]
    for gift in gifts:
        gift.start()
    for part in range(3):
        xblk[at[ORDERS[part][0]], :, cols_of(part)] = hid_ref[:, cols_of(part)]
    href = lambda line, part: hall.at[line, :, cols_of(part)]
    hidden_lines = (ep, tp, at, href, s2, r2, s3, r3)
    for part in range(3):
        first_arrived(ep, tp, at, part, own(part), slot(part), s1, r1)
        off, width = PARTS[part]
        for n in range(off, off + width, 128):
            cols = pl.ds(n, 128)
            hall[line_of(at, part, 0, 0), :, cols] = stacked([xblk[c, :, cols].astype(F32) for c in range(4)], (0, 2))
        lines_early((part,), *hidden_lines)
    for load in loads:
        load.wait()
    squares[...] = jnp.zeros((128, 128), F32)
    for t in range(2):
        weights[pl.ds(t, 64, stride=2), :] = jnp.where(
            tp == 0, recv_ref[pl.ds(t, 64, stride=4), :], recv_ref[pl.ds(2 + t, 64, stride=4), :]
        )
    for line, row, line_t, row_t in turned_pieces():
        a0, b0 = 8 * line + row, 8 * line_t + row_t
        weights_t[b0 : b0 + 2, :] = weights[a0 : a0 + 2, :]
    r = lax.broadcasted_iota(jnp.int32, (128, 128), 0)
    c = lax.broadcasted_iota(jnp.int32, (128, 128), 1)
    turn = (c == (r // 32) * 32 + (r // 2 % 4) * 8 + (r // 8 % 4) * 2 + r % 2).astype(BF16)
    lines_late((0, 1, 2), *hidden_lines)

    def onto(off, width):
        left = hall[:, :, pl.ds(off, width)].reshape(256, width)
        return lax.dot_general(left, wo[:, pl.ds(off, width)], (((1,), (1,)), ((), ())), preferred_element_type=F32)

    pre[...] = onto(0, TURN).reshape(16, 16, 64)
    pre_t[...] = onto(TURN, 768).reshape(16, 16, 64)
    for core in range(2):
        for line, row, line_t, row_t in turned_pieces():
            a0, b0 = 8 * core + row, 8 * core + row_t
            pre[line, a0 : a0 + 2] += pre_t[line_t, b0 : b0 + 2]
        sides = [pre[8 * k : 8 * k + 8, 8 * core : 8 * core + 8].reshape(64, 64) for k in range(2)]
        pk[core] = jnp.concatenate(sides, axis=1).astype(BF16)
    swap = remote(pk.at[1 - tp], pr_in, hs, hr, ep, 1 - tp)
    swap.start()
    for part in range(3):
        first_end(ep, tp, at, part, own(part), slot(part), s1, r1)
    lines_end((0, 1, 2), *hidden_lines)
    swap.wait()
    mine = at["z"] * 4 + at["y"]
    mall[mine, at["x"]] = (pk[tp].astype(F32) + pr_in[...].astype(F32)).astype(BF16)
    both = (0, 1)
    mown = lambda part: mall.at[mine, at["x"], pl.ds(32 * part, 32), :]
    mslot = lambda part: lambda c: mall.at[mine, c, pl.ds(32 * part, 32), :]
    for part in both:
        first_send(ep, tp, at, part, mown(part), mslot(part), ms1, mr1)
    mref = lambda line, part: mall.at[line, :, pl.ds(32 * part, 32), :]
    mixed_lines = (ep, tp, at, mref, ms2, mr2, ms3, mr3)
    for part in both:
        first_arrived(ep, tp, at, part, mown(part), mslot(part), ms1, mr1)
        lines_early((part,), *mixed_lines)

    low = lax.broadcasted_iota(jnp.int32, (32, 128), 1) < 64

    def joined(part, line):
        rows = [slice(64 * k + 32 * part, 64 * k + 32 * part + 32) for k in range(2)]
        total = [squares[rows[k], :] for k in range(2)]
        for i in range(2):
            a = mall[line, 2 * i, 32 * part : 32 * part + 32, :].astype(F32)
            b = mall[line, 2 * i + 1, 32 * part : 32 * part + 32, :].astype(F32)
            mixes = (jnp.where(low, a, pltpu.roll(b, 64, 1)), jnp.where(low, pltpu.roll(a, 64, 1), b))
            cols = pl.ds(pl.multiple_of(256 * line + 128 * i, 128), 128)
            for k in range(2):
                first = 8 * k + 4 * part
                summed = toks[first : first + 4, :, cols].astype(F32).reshape(32, 128) + mixes[k]
                resid[rows[k], cols] = summed
                total[k] += summed * summed
        for k in range(2):
            squares[rows[k], :] = total[k]

    lines_late(both, *mixed_lines, seen=joined)
    scale = lax.rsqrt(jnp.sum(squares[...], axis=-1, keepdims=True) * (1.0 / 4096) + 1e-06)
    for n in range(3):
        gifts[n].wait_send()
        remote(wg_hbm, shared[n][1].at[1 - tp], es.at[n], er.at[n], ep, 1 - tp).wait_recv()
    for n in range(0, 4096, 1024):
        cols = pl.ds(n, 1024)
        x = (resid[:, cols] * scale * gain_ref[:, cols]).astype(BF16)
        for k in range(2):
            g = jnp.dot(x, wg[k, cols, :], preferred_element_type=F32)
            u = jnp.dot(x, wu[k, cols, :], preferred_element_type=F32)
            if n == 0:
                gate[k] = g
                up[k] = u
            else:
                gate[k] += g
                up[k] += u
    for k in range(2):
        g = gate[k]
        act[k] = (g * jax.nn.sigmoid(g) * up[k]).astype(BF16)
        act_t[k] = jnp.dot(turn, act[k], preferred_element_type=F32).astype(BF16)

    r1_at = lambda part, o: r1buf.at[part, o, :, :, pl.ds(0, WIDE[part][1])]
    for part in (2, 0, 1):
        off, width = WIDE[part]
        left, by = (act_t, weights_t) if part == 2 else (act, weights)
        for n in range(off, off + width, 256):
            cols = pl.ds(n, 256)
            t0 = jnp.dot(left[0], wd[0, :, cols], preferred_element_type=F32).astype(BF16).astype(F32)
            t1 = jnp.dot(left[1], wd[1, :, cols], preferred_element_type=F32).astype(BF16).astype(F32)
            terms[:, :, :, cols] = ((t0 + t1) * by[:, 96:97]).reshape(4, 4, 8, 256).astype(BF16)
        axis = ORDERS[part][2]
        for o in SEND_ORDER:
            k = shifted(at, axis, o)
            src = terms.at[k, :, :, wide_of(part)] if part == 0 else terms.at[:, k, :, wide_of(part)]
            remote(src, r1_at(part, o), q1s.at[part, o], q1r.at[part, o], peer(ep, at, axis, o), tp).start()
    for part in both:
        first_end(ep, tp, at, part, mown(part), mslot(part), ms1, mr1)
    lines_end(both, *mixed_lines)

    s1_at = lambda part, k: s1buf.at[part, k, :, pl.ds(0, WIDE[part][1])]
    r2_at = lambda part, o: r2buf.at[part, o, :, pl.ds(0, WIDE[part][1])]
    for part in (2, 0, 1):
        off, width = WIDE[part]
        for o in SEND_ORDER:
            remote(r1_at(part, 0), r1_at(part, o), q1s.at[part, o], q1r.at[part, o], ep, tp).wait_recv()
        for n in range(0, width, 256):
            cols = pl.ds(off + n, 256)
            mine_term = terms[at["z"], :, :, cols] if part == 0 else terms[:, at[ORDERS[part][2]], :, cols]
            total = mine_term.astype(F32)
            for o in (1, 2, 3):
                total += r1buf[part, o, :, :, pl.ds(n, 256)].astype(F32)
            s1buf[part, :, :, pl.ds(n, 256)] = total.astype(BF16)
        axis = ORDERS[part][1]
        for o in SEND_ORDER:
            remote(s1_at(part, shifted(at, axis, o)), r2_at(part, o), q2s.at[part, o], q2r.at[part, o], peer(ep, at, axis, o), tp).start()
    for part in (2, 0, 1):
        off, width = WIDE[part]
        for o in SEND_ORDER:
            remote(s1_at(part, 0), r2_at(part, o), q2s.at[part, o], q2r.at[part, o], ep, tp).wait_recv()
        for n in range(0, width, 256):
            total = s1buf[part, at[ORDERS[part][1]], :, pl.ds(n, 256)].astype(F32)
            for o in (1, 2, 3):
                total += r2buf[part, o, :, pl.ds(n, 256)].astype(F32)
            for k in range(4):
                xsend[k, :, pl.ds(off + n, 256)] = total[2 * k : 2 * k + 2].astype(BF16)
        axis = ORDERS[part][0]
        for o in SEND_ORDER:
            there = xsend.at[shifted(at, axis, o), :, wide_of(part)]
            remote(there, xrecv.at[o, :, wide_of(part)], q3s.at[part, o], q3r.at[part, o], peer(ep, at, axis, o), tp).start()
    for part in (2, 0, 1):
        off, width = WIDE[part]
        cols = wide_of(part)
        eight = resid[pl.ds(pl.multiple_of(8 * mine, 8), 8), cols]
        total = eight[0:2]
        for k in range(1, 4):
            total = jnp.where(at["x"] == k, eight[2 * k : 2 * k + 2], total)
        total = total + xsend[at[ORDERS[part][0]], :, cols].astype(F32)
        for o in SEND_ORDER:
            remote(xsend.at[0, :, cols], xrecv.at[o, :, cols], q3s.at[part, o], q3r.at[part, o], ep, tp).wait_recv()
            total += xrecv[o, :, cols].astype(F32)
        ends[tp, :, cols] = total.astype(BF16)
    last = remote(ends.at[tp], ends.at[tp], fs, fr, ep, 1 - tp)
    last.start()
    for part in range(3):
        for o in SEND_ORDER:
            remote(r1_at(part, 0), r1_at(part, o), q1s.at[part, o], q1r.at[part, o], ep, tp).wait_send()
            remote(s1_at(part, 0), r2_at(part, o), q2s.at[part, o], q2r.at[part, o], ep, tp).wait_send()
            there = xsend.at[0, :, wide_of(part)]
            remote(there, xrecv.at[o, :, wide_of(part)], q3s.at[part, o], q3r.at[part, o], ep, tp).wait_send()
    last.wait_send()
    remote(ends.at[1 - tp], ends.at[1 - tp], fs, fr, ep, 1 - tp).wait_recv()
    for n in range(0, 4096, 1024):
        cols = pl.ds(n, 1024)
        out_ref[:, cols] = jnp.concatenate([ends[k, :, cols].astype(F32) for k in range(2)], axis=0).astype(BF16)


V = pl.BlockSpec(memory_space=pltpu.VMEM)
ANY = pl.BlockSpec(memory_space=pl.ANY)
DMA = pltpu.SemaphoreType.DMA


def shape(dims, dtype):
    return jax.ShapeDtypeStruct(dims, dtype)


def call_a(tokens, gain, ids, rw, wq, wk, wv, wo):
    return pl.pallas_call(
        kernel_a,
        name="gather_project",
        out_shape=(shape((64, 4, 128), F32), shape((16, 8, 4096), BF16)),
        in_specs=[V, V, V, V, ANY, ANY, ANY, ANY],
        out_specs=(V, V),
        scratch_shapes=[
            pltpu.VMEM((2, 4096), BF16),
            pltpu.VMEM((4, 2, 4096), BF16),
            pltpu.VMEM((4, 4, 4096), BF16),
            pltpu.VMEM((4, 4, 4096), BF16),
            pltpu.VMEM((4, 8, 4096), BF16),
            pltpu.VMEM((4, 8, 4096), BF16),
            pltpu.VMEM((2, 128, 4096), BF16),
            pltpu.VMEM((128, 256), F32),
            pltpu.VMEM((128, 256), F32),
            pltpu.VMEM((16, 8, 128), F32),
            pltpu.VMEM((16, 8, 128), F32),
            pltpu.VMEM((2, 64, 2, 128), F32),
            pltpu.VMEM((64, 2, 128), F32),
            pltpu.VMEM((64, 4, 128), F32),
            DMA((4,)),
            DMA((3, 4)), DMA((3, 4)),
            DMA((3, 4)), DMA((3, 4)),
            DMA((3, 4, 4)), DMA((3, 4, 4)),
            DMA(()), DMA(()), DMA(()), DMA(()),
            DMA((64,)), DMA((64,)),
        ],
        compiler_params=pltpu.CompilerParams(collective_id=0, has_side_effects=True),
        cost_estimate=pl.CostEstimate(flops=10**9, bytes_accessed=10**7, transcendentals=0),
    )(tokens, gain, ids, rw, wq, wk, wv, wo)


def call_b(recv, tokens, gain, win, wfg, fbias, stab, nrm, mem):
    return pl.pallas_call(
        kernel_b,
        name="cell",
        out_shape=(
            shape(mem.shape, F32), shape(nrm.shape, F32), shape(stab.shape, F32), shape((4, 2048), BF16),
        ),
        in_specs=[V, V, V, V, V, V, V, V, ANY],
        out_specs=(ANY, V, V, V),
        scratch_shapes=[
            pltpu.VMEM((16, 256, 512), F32),
            pltpu.VMEM((16, 256, 256), F32),
            pltpu.VMEM((4, 2048), F32),
            DMA((16,)), DMA((16,)),
        ],
        compiler_params=pltpu.CompilerParams(),
        cost_estimate=pl.CostEstimate(flops=10**8, bytes_accessed=2 * 10**7, transcendentals=0),
    )(recv, tokens, gain, win, wfg, fbias, stab, nrm, mem)


def call_c(hidden, recv, gain, gathered, wo, wg, wu, wd):
    lines = lambda k: [DMA((k, 4)), DMA((k, 4)), DMA((k, 4)), DMA((k, 4)), DMA((k, 4, 4)), DMA((k, 4, 4))]
    return pl.pallas_call(
        kernel_c,
        name="experts",
        out_shape=shape((4, 4096), BF16),
        in_specs=[V, V, V, ANY, ANY, ANY, ANY, ANY],
        out_specs=V,
        scratch_shapes=[
            pltpu.VMEM((4, 4, 2048), BF16),
            pltpu.VMEM((16, 16, 2048), BF16),
            pltpu.VMEM((64, 2048), BF16),
            pltpu.VMEM((16, 8, 4096), BF16),
            pltpu.VMEM((2, 4096, 256), BF16),
            pltpu.VMEM((2, 4096, 256), BF16),
            pltpu.VMEM((2, 256, 4096), BF16),
            pltpu.VMEM((16, 16, 64), F32),
            pltpu.VMEM((16, 16, 64), F32),
            pltpu.VMEM((2, 64, 128), BF16),
            pltpu.VMEM((64, 128), BF16),
            pltpu.VMEM((16, 4, 64, 128), BF16),
            pltpu.VMEM((128, 4096), F32),
            pltpu.VMEM((128, 128), F32),
            pltpu.VMEM((2, 128, 256), F32),
            pltpu.VMEM((2, 128, 256), F32),
            pltpu.VMEM((2, 128, 256), BF16),
            pltpu.VMEM((2, 128, 256), BF16),
            pltpu.VMEM((128, 128), F32),
            pltpu.VMEM((128, 128), F32),
            pltpu.VMEM((4, 4, 8, 4096), BF16),
            pltpu.VMEM((3, 4, 4, 8, 1536), BF16),
            pltpu.VMEM((3, 4, 8, 1536), BF16),
            pltpu.VMEM((3, 4, 8, 1536), BF16),
            pltpu.VMEM((4, 2, 4096), BF16),
            pltpu.VMEM((4, 2, 4096), BF16),
            pltpu.VMEM((2, 2, 4096), BF16),
            DMA((5,)),
            *lines(3),
            *lines(2), DMA((3,)), DMA((3,)),
            DMA(()), DMA(()),
            DMA((3, 4)), DMA((3, 4)), DMA((3, 4)), DMA((3, 4)), DMA((3, 4)), DMA((3, 4)), DMA(()), DMA(()),
        ],
        compiler_params=pltpu.CompilerParams(collective_id=1, has_side_effects=True),
        cost_estimate=pl.CostEstimate(flops=2 * 10**9, bytes_accessed=10**7, transcendentals=0),
    )(hidden, recv, gain, gathered, wo, wg, wu, wd)


def body(
    tokens, memory, normalizer, stabilizer, norm_gain, w_query, w_key, w_value, w_outgate, w_input, w_forget,
    forget_bias, w_out, ffn_gain, w_gate, w_up, w_down, expert_ids, route_weights,
):
    turned = lambda w: jnp.transpose(w, (1, 2, 0))
    gain = norm_gain.reshape(1, -1)
    recv, gathered = call_a(
        tokens, gain, expert_ids.T, route_weights.T, turned(w_query), turned(w_key), turned(w_value), turned(w_outgate)
    )
    flat = recv.reshape(256, 128)
    memory_next, normalizer_next, stab_next, hidden = call_b(
        flat, tokens, gain, w_input.T, w_forget.T, forget_bias.reshape(1, 4), stabilizer, normalizer, memory
    )
    out = call_c(hidden, flat, ffn_gain.reshape(1, -1), gathered, w_out.T, w_gate[0], w_up[0], w_down[0])
    return (out, memory_next, normalizer_next, stab_next)


def solution(mesh):
    return jax.shard_map(
        body,
        mesh=mesh,
        in_specs=(
            P("ep", None),
            P("ep", "tp", None, None),
            P("ep", "tp", None),
            P("ep", "tp"),
            P(),
            P(None, "tp", "ep"),
            P(None, "tp", "ep"),
            P(None, "tp", "ep"),
            P(None, "tp", "ep"),
            P(None, "tp"),
            P(None, "tp"),
            P("tp"),
            P("tp", "ep"),
            P(),
            P("ep", None, "tp"),
            P("ep", None, "tp"),
            P("ep", "tp", None),
            P("ep", None),
            P("ep", None),
        ),
        out_specs=(P("ep", None), P("ep", "tp", None, None), P("ep", "tp", None), P("ep", "tp")),
        check_vma=False,
    )
```

time: 110 us -> 97 us (0.88)
  Pallas kernels: 107 us -> 94.7 us
    pallas_call x1, Pallas kernels: 63.1 us -> 53.6 us  [call_c(): pl.pallas_call(kernel_c, name='experts', out_shape=shape((4, 4096), BF16)...]
    pallas_call x1, Pallas kernels: 10.1 us -> 7.75 us  [call_b(): pl.pallas_call(kernel_b, name='cell', out_shape=(shape(mem.shape, F32), s...]
where the time goes in v2:
time: 97 us; the launch traced here: 96.7 us
  Pallas kernels  94.7 us (98%)
  local copies, waits for them, and re-layouts  1.39 us (1%)
    pallas_call x1, Pallas kernels, call_c(): pl.pallas_call(kernel_c, name='experts', out_shape=shape((4, 4096), BF16)...  53.6 us
    pallas_call x1, Pallas kernels, call_a(): pl.pallas_call(kernel_a, name='gather_project', out_shape=(shape((64, 4,...  33.3 us
    pallas_call x1, Pallas kernels, call_b(): pl.pallas_call(kernel_b, name='cell', out_shape=(shape(mem.shape, F32), s...  7.75 us

profile of v2, /device:TPU:1, one launch (start us, length us, event | category | flops | bytes accessed | tf_op | source)
XLA Modules:
  0.0 96.7 jit_solution(15776046536649120960)
XLA Ops:
  0.6 33.3 %gather_project.1 = (f32[64,4,128]{2,1,0:T(4,128)}, bf16[16,8,4096]{2,1,0:T(8,128)(2,1)}) custom-call(bf16[4,4096]{1,0:T(4,128)(2,1)} %tok_ref.3, f32[1,4096]{1,0:T(1,128)} %bitcast.24, s32[2,4]{1,0:T(2,128)} %bitcast.32, f32[2,4]{1,0:T(2,128)} %bitcast.33, bf16[4,4,4096]{2,1,0:T(4,128)(2,1)} %bitcast.30, bf16[4,4,4096]{2,1,0:T(4,128)(2,1)} %bitcast.31, ...), custom_call_target="tpu_custom_call" | custom-call | flops 1000000000 | bytes 10000000 | tf_op jit(solution)/shard_map/gather_project/pallas_call | solution.py:583
  34.0 7.7 %cell.1 = (f32[4,4,256,512]{3,2,1,0:T(8,128)}, f32[4,4,256]{2,1,0:T(4,128)}, f32[4,4]{1,0:T(4,128)}, bf16[4,2048]{1,0:T(4,128)(2,1)}) custom-call(f32[256,128]{1,0:T(8,128)} %bitcast.19, bf16[4,4096]{1,0:T(4,128)(2,1)} %tok_ref.3, f32[1,4096]{1,0:T(1,128)} %bitcast.25, bf16[4,4096]{1,0:T(4,128)(2,1)} %bitcast.22, bf16[4,4096]{1,0:T(4,128)(2,1)} %bitcast.23, ...), custom_call_target="tpu_custom_call" | custom-call | flops 100000000 | bytes 20000000 | tf_op jit(solution)/shard_map/cell/pallas_call | solution.py:617
  41.7 53.6 %experts.1 = bf16[4,4096]{1,0:T(4,128)(2,1)} custom-call(bf16[4,2048]{1,0:T(4,128)(2,1)} %get-tuple-element.11.hid_ref, f32[256,128]{1,0:T(8,128)} %bitcast.20, f32[1,4096]{1,0:T(1,128)} %bitcast.26, bf16[16,8,4096]{2,1,0:T(8,128)(2,1)} %get-tuple-element.12.tok_hbm, bf16[64,2048]{1,0:T(8,128)(2,1)} %bitcast.21, bf16[4096,256]{1,0:T(8,128)(2,1)} %bitcast.16, ...), custom_call_target="tpu_custom_call" | custom-call | flops 2000000000 | bytes 10000000 | tf_op jit(solution)/shard_map/experts/pallas_call | solution.py:638
  95.3 1.4 %copy.24 = bf16[4,4096]{1,0:T(4,128)(2,1)} copy(bf16[4,4096]{1,0:T(4,128)(2,1)} %experts.1) | data formatting | bytes 65536
